TPU v7x, 32 devices: a whole 2x2x4 slice. The times are simulated.
32 devices in a mesh: kv: 4 (over y, x), tp: 8 (over z, core).
Axes of the slice: x: 2, y: 2, z: 4, core: 2. Of those that a mesh axis runs over, the one named last changes fastest.
Arguments:
- stream: bfloat16 [32, 4096], P(None, ('kv', 'tp')), may hold values from -18 to 18
- mixer_gain: float32 [4096], replicated, may hold values from 0.1 to 1.9
- query_weight: bfloat16 [4096, 1024], P(None, 'tp'), may hold values from -0.09375 to 0.09375
- key_weight: bfloat16 [4096, 1024], P(None, 'tp'), may hold values from -0.09375 to 0.09375
- value_weight: bfloat16 [4096, 1024], P(None, 'tp'), may hold values from -0.09375 to 0.09375
- forget_weight: bfloat16 [4096, 16], replicated, may hold values from -0.09375 to 0.09375
- forget_bias: float32 [16], replicated, may hold values from -4 to -2
- key_cache: bfloat16 [32, 16, 4096, 64], P(None, 'tp', 'kv'), may hold values from -512 to 512, as said below
- value_cache: bfloat16 [32, 16, 4096, 64], P(None, 'tp', 'kv'), may hold values from -12 to 12
- past_decay: float32 [32, 16, 4096], P(None, 'tp', 'kv'), may hold values from -4096 to 0, as said below
- out_weight: bfloat16 [1024, 4096], P('tp', 'kv'), may hold values from -0.75 to 0.75
- channel_gain: float32 [4096], replicated, may hold values from 0.1 to 1.9
- up_weight: bfloat16 [4096, 16384], P('kv', 'tp'), may hold values from -0.09375 to 0.09375
- down_weight: bfloat16 [16384, 4096], P('tp', 'kv'), may hold values from -0.0625 to 0.0625
Outputs:
- updated: bfloat16 [32, 4096], P(None, ('kv', 'tp'))
Inputs may be any that keep to these rules, and one draw needn't show every extreme that they name: `key_cache`: keys of order one; some cached keys may be much larger. `past_decay`: never falling along the positions of a sequence and head, zero at the last cached position.
All inputs are finite; a program needn't handle non-finite values.
Results may differ from a plain program's by a relative error of at most 0.014.
The roundings to bfloat16 on the way count: a program that leaves them out, or rounds other values in their place, can miss the bound.
Values may be sent and summed in bfloat16 or wider, within the bound.
No kernel may reach another device: no remote copies, remote signals or barrier semaphores. Data moves between devices by JAX's collectives and lax.ppermute only.
A program may use at most 64 MiB of HBM per device.

v0:
```python
import jax
import jax.numpy as jnp
from jax import lax
from jax.sharding import PartitionSpec as P

D = 4096


EPS = 1e-06


def combined_all(part, axis, combine):
    gathered = jax.tree.map(lambda a: lax.all_gather(a, axis), part)

    def take(source):
        return jax.tree.map(lambda a: lax.dynamic_index_in_dim(a, source, 0, False), gathered)

    return lax.fori_loop(
        1, lax.axis_size(axis), lambda source, state: combine(state, take(source)), take(0)
    )


def rms_scale(values, gain):
    widened = values.astype(jnp.float32)
    inverse = lax.rsqrt(jnp.mean(widened * widened, axis=-1, keepdims=True) + EPS)
    return (widened * inverse * gain).astype(jnp.bfloat16)


def merge_parts(earlier, later):
    top_one, total_one, sums_one = earlier
    top_two, total_two, sums_two = later
    highest = jnp.maximum(top_one, top_two)
    factor_one = jnp.exp(top_one - highest)
    factor_two = jnp.exp(top_two - highest)
    return (
        highest,
        total_one * factor_one + total_two * factor_two,
        sums_one * factor_one[..., None] + sums_two * factor_two[..., None],
    )


def squared_relu(values):
    return jnp.square(jax.nn.relu(values)).astype(jnp.bfloat16)


def row_squares(values):
    widened = values.astype(jnp.float32)
    return jnp.sum(widened * widened, axis=1)


def shards(
    stream,
    mixer_gain,
    query_weight,
    key_weight,
    value_weight,
    forget_weight,
    forget_bias,
    key_cache,
    value_cache,
    past_decay,
    out_weight,
    channel_gain,
    up_weight,
    down_weight,
):
    batch_rows = stream.shape[0]
    local_heads = key_cache.shape[1]
    head_size = key_cache.shape[3]
    scale_factor = float(head_size) ** (-0.5)
    gathered = lax.all_gather(stream, ("kv", "tp"), axis=1, tiled=True)
    normed = rms_scale(gathered, mixer_gain)
    queries = jnp.dot(normed, query_weight, preferred_element_type=jnp.float32).astype(jnp.bfloat16)
    keys_new = jnp.dot(normed, key_weight, preferred_element_type=jnp.float32).astype(jnp.bfloat16)
    values_new = jnp.dot(normed, value_weight, preferred_element_type=jnp.float32).astype(
        jnp.bfloat16
    )
    forget_all = jax.nn.log_sigmoid(
        jnp.dot(normed, forget_weight, preferred_element_type=jnp.float32) + forget_bias
    )
    forget = lax.dynamic_slice_in_dim(
        forget_all, lax.axis_index("tp") * local_heads, local_heads, 1
    )
    query_heads = queries.reshape(batch_rows, local_heads, head_size)
    scores = (
        jnp.einsum("bhd,bhpd->bhp", query_heads, key_cache, preferred_element_type=jnp.float32)
        * scale_factor
        + forget[..., None]
        + past_decay
    )
    highest = jnp.max(scores, axis=-1)
    weights = jnp.exp(scores - highest[..., None]).astype(jnp.bfloat16)
    totals = jnp.sum(weights.astype(jnp.float32), axis=-1)
    sums = jnp.einsum("bhp,bhpd->bhd", weights, value_cache, preferred_element_type=jnp.float32)
    highest, totals, sums = combined_all((highest, totals, sums), "kv", merge_parts)
    key_heads = keys_new.reshape(batch_rows, local_heads, head_size).astype(jnp.float32)
    value_heads = values_new.reshape(batch_rows, local_heads, head_size).astype(jnp.float32)
    own = jnp.sum(query_heads.astype(jnp.float32) * key_heads, axis=-1) * scale_factor
    peak = jnp.maximum(highest, own)
    cache_factor = jnp.exp(highest - peak)
    own_factor = jnp.exp(own - peak)
    numer = sums * cache_factor[..., None] + value_heads * own_factor[..., None]
    denom = totals * cache_factor + own_factor
    attention = (
        (numer / denom[..., None]).astype(jnp.bfloat16).reshape(batch_rows, local_heads * head_size)
    )
    partial_value = jnp.dot(attention, out_weight, preferred_element_type=jnp.float32)
    piece_width = stream.shape[1]
    block_width = partial_value.shape[1]
    block_sum = lax.psum(partial_value, "tp")
    own_block = lax.dynamic_slice_in_dim(
        gathered, lax.axis_index("kv") * block_width, block_width, 1
    )
    middle_block = (own_block.astype(jnp.float32) + block_sum).astype(jnp.bfloat16)
    squares = lax.psum(row_squares(middle_block), "kv")
    middle_piece = lax.dynamic_slice_in_dim(
        middle_block, lax.axis_index("tp") * piece_width, piece_width, 1
    )
    inverse = lax.rsqrt(squares / D + EPS)
    gain_block = lax.dynamic_slice_in_dim(
        channel_gain, lax.axis_index("kv") * block_width, block_width, 0
    )
    mixed_block = (
        middle_block.astype(jnp.float32) * inverse[:, None] * gain_block[None, :]
    ).astype(jnp.bfloat16)
    up_partial = jnp.dot(mixed_block, up_weight, preferred_element_type=jnp.float32)
    hidden = squared_relu(lax.psum(up_partial, "kv"))
    down_partial = jnp.dot(hidden, down_weight, preferred_element_type=jnp.float32)
    reduced = lax.psum_scatter(down_partial, "tp", scatter_dimension=1, tiled=True)
    return (middle_piece.astype(jnp.float32) + reduced).astype(jnp.bfloat16)


def solution(mesh):
    return jax.shard_map(
        shards,
        mesh=mesh,
        in_specs=(
            P(None, ("kv", "tp")),
            P(),
            P(None, "tp"),
            P(None, "tp"),
            P(None, "tp"),
            P(),
            P(),
            P(None, "tp", "kv", None),
            P(None, "tp", "kv", None),
            P(None, "tp", "kv"),
            P("tp", "kv"),
            P(),
            P("kv", "tp"),
            P("tp", "kv"),
        ),
        out_specs=P(None, ("kv", "tp")),
        check_vma=False,
    )
```

profile of v0, /device:TPU:0, one launch (start us, length us, event | category | flops | bytes accessed | tf_op | source)
XLA Modules:
  0.0 247.9 jit_solution(13276194251928122677)
XLA Ops:
  6.5 44.6 %all_gather.21 = bf16[32,4096]{1,0:T(8,128)(2,1)S(1)} all-gather(bf16[32,128]{1,0:T(8,128)(2,1)} %param.16), channel_id=1, replica_groups=mesh['kv'=4,'tp'=8] {'kv','tp'}, dimensions={1}, use_global_device_ids=true | all-gather | bytes 270336 | tf_op jit(solution)/shard_map/all_gather | solution.py:71
  51.4 1.0 convolution_convert_fusion.2
  52.6 1.2 fusion.40
  53.9 4.6 %fusion.41 = f32[32,2,1,1024]{3,2,1,0:T(1,128)S(1)} fusion(bf16[32,2,64,1]{2,3,1,0:T(2,128)(2,1)S(1)} %reshape.57, bf16[32,2,1024,64]{2,3,1,0:T(8,128)(2,1)} %param.23), kind=kOutput, calls=%fused_computation.63 | convolution fusion | flops 8388608 | bytes 8658944 | tf_op jit(solution)/shard_map/bhd,bhpd->bhp/dot_general | solution.py:86
  58.5 2.1 fusion.38
  60.6 1.3 fusion.30
  61.9 5.7 %fusion.11 = f32[32,2,1,64]{3,2,1,0:T(1,128)S(1)} fusion(bf16[32,2,1024,64]{2,3,1,0:T(8,128)(2,1)} %param.24, bf16[32,2,1024,1]{2,1,0,3:T(2,128)(2,1)S(1)} %get-tuple-element.211), kind=kOutput, calls=%fused_computation.24 | convolution fusion | flops 8388608 | bytes 8536064 | tf_op jit(solution)/shard_map/bhp,bhpd->bhd/dot_general | solution.py:94
  67.6 7.5 %all-gather.2 = f32[128,2,64]{2,1,0:T(2,128)S(1)} all-gather(f32[32,2,64]{2,1,0:T(2,128)S(1)} %bitcast.49), channel_id=4, replica_groups=mesh['kv'=4,'tp'=8] {'kv'}, dimensions={0}, use_global_device_ids=true | all-gather | bytes 81920 | tf_op jit(solution)/shard_map/all_gather | solution.py:13
  75.8 8.1 %all-gather.4 = f32[4,32,2]{1,2,0:T(2,128)S(1)} all-gather(f32[1,32,2]{1,2,0:T(2,128)S(1)} %bitcast.51), channel_id=3, replica_groups=mesh['kv'=4,'tp'=8] {'kv'}, dimensions={0}, use_global_device_ids=true | all-gather | bytes 1280 | tf_op jit(solution)/shard_map/all_gather | solution.py:13
  83.8 7.1 %all-gather.3 = f32[4,32,2]{1,2,0:T(2,128)S(1)} all-gather(f32[1,32,2]{1,2,0:T(2,128)S(1)} %bitcast.50), channel_id=2, replica_groups=mesh['kv'=4,'tp'=8] {'kv'}, dimensions={0}, use_global_device_ids=true | all-gather | bytes 1280 | tf_op jit(solution)/shard_map/all_gather | solution.py:13
  90.9 3.6 %while.19 = (s32[]{:T(128)}, f32[32,2]{0,1:T(2,128)S(1)}, f32[32,2]{0,1:T(2,128)S(1)}, f32[32,2,64]{2,1,0:T(2,128)S(1)}, f32[4,32,2]{1,2,0:T(2,128)S(1)}, /*inde...) while((s32[]{:T(128)}, f32[32,2]{0,1:T(2,128)S(1)}, ...), condition=%wide.region_4.5_spmd, body=%wide.region_3.4_spmd.sunk | while | flops 12677 | bytes 52887 | solution.py:18
  91.1 1.0 fusion.57
  92.3 1.0 fusion.57
  93.5 1.0 fusion.57
  96.2 1.8 fusion.42
  98.0 0.7 dynamic_slice.59
  98.7 51.7 %all-reduce.3.cloned.1.call-done = f32[32,1024]{1,0:T(8,128)} async-done(((f32[32,1024]{1,0:T(8,128)}), f32[32,1024]{1,0:T(8,128)}) %all-reduce.3.cloned.1.call-update) | async-done | bytes 131088 | tf_op jit(solution)/shard_map/psum | solution.py:110
  150.4 1.0 fusion.13
  151.4 9.8 %psum.22 = f32[32]{0:T(128)S(1)} all-reduce(f32[32]{0:T(128)S(1)} %get-tuple-element.204), channel_id=1, replica_groups=mesh['kv'=4,'tp'=8] {'kv'}, use_global_device_ids=true, to_apply=%region_8.9 | all-reduce | flops 32 | bytes 256 | tf_op jit(solution)/shard_map/psum | solution.py:115
  161.3 3.8 %fusion.18 = f32[32,2048]{1,0:T(8,128)} fusion(bf16[1024,2048]{1,0:T(8,128)(2,1)} %param.28, bf16[32,1024]{1,0:T(8,128)(2,1)S(1)} %get-tuple-element.205, f32[1024]{0:T(1024)S(1)} %dynamic_slice.59, f32[32]{0:T(128)S(1)} %add_rsqrt_fusion), kind=kOutput, calls=%fused_computation.37 | convolution fusion | flops 134348800 | bytes 4526208 | tf_op jit(solution)/shard_map/dot_general | solution.py:126
  165.1 40.4 %all-reduce.5.cloned.1.call-done = f32[32,2048]{1,0:T(8,128)} async-done(((f32[32,2048]{1,0:T(8,128)}), f32[32,2048]{1,0:T(8,128)}) %all-reduce.5.cloned.1.call-update) | async-done | bytes 262160 | tf_op jit(solution)/shard_map/psum | solution.py:127
  205.5 3.8 %fusion.16 = f32[32,1024]{1,0:T(8,128)} fusion(bf16[2048,1024]{1,0:T(8,128)(2,1)} %param.29, f32[32,2048]{1,0:T(8,128)} %all-reduce.5.cloned.1.call-done), kind=kOutput, calls=%fused_computation.34 | convolution fusion | flops 134414336 | bytes 4587520 | tf_op jit(solution)/shard_map/dot_general | solution.py:128
  209.3 30.7 %reduce-scatter.2.cloned.1.call-done = f32[32,128]{1,0:T(8,128)} async-done(((f32[32,1024]{1,0:T(8,128)}), f32[32,128]{1,0:T(8,128)}) %reduce-scatter.2.cloned.1.call-update) | async-done | bytes 16400 | tf_op jit(solution)/shard_map/reduce_scatter | solution.py:129
  240.0 1.3 add_convert_fusion.1
  (49 shorter events, 3.6 us)
Async XLA Ops:
  6.5 44.8 %copy-start = (bf16[4096,128]{1,0:T(8,128)(2,1)S(1)}, bf16[4096,128]{1,0:T(8,128)(2,1)}, u32[]{:S(2)}) copy-start(bf16[4096,128]{1,0:T(8,128)(2,1)} %param.18) | copy-start | bytes 3145732
  6.5 143.8 %all-reduce.3.cloned.1.call-start = ((), (), s32[]{:S(2)}) async-start(), calls=%async_computation.1 | async-start | bytes 262144 | tf_op jit(solution)/shard_map/psum | solution.py:110
  58.4 36.1 %copy-start.1 = (bf16[4096,128]{1,0:T(8,128)(2,1)S(1)}, bf16[4096,128]{1,0:T(8,128)(2,1)}, u32[]{:S(2)}) copy-start(bf16[4096,128]{1,0:T(8,128)(2,1)} %param.19) | copy-start | bytes 3145732
  58.4 36.1 %copy-start.4 = (f32[4096]{0:T(1024)S(1)}, f32[4096]{0:T(1024)}, u32[]{:S(2)}) copy-start(f32[4096]{0:T(1024)} %param.17) | copy-start | bytes 49156
  58.5 37.0 %copy-start.2 = (bf16[4096,128]{1,0:T(8,128)(2,1)S(1)}, bf16[4096,128]{1,0:T(8,128)(2,1)}, u32[]{:S(2)}) copy-start(bf16[4096,128]{1,0:T(8,128)(2,1)} %param.20) | copy-start | bytes 3145732
  75.0 0.6 copy-start.3
  98.0 107.5 %all-reduce.5.cloned.1.call-start = ((), (), s32[]{:S(2)}) async-start(), calls=%async_computation.2 | async-start | bytes 524288 | tf_op jit(solution)/shard_map/psum | solution.py:127
  165.1 75.0 %reduce-scatter.2.cloned.1.call-start = ((), (), s32[]{:S(2)}) async-start(), calls=%async_computation.3 | async-start | bytes 147456 | tf_op jit(solution)/shard_map/reduce_scatter | solution.py:129
Sparse Core Ops, SparseCore 0:
  98.1 52.2 all-reduce.2
  165.2 40.2 all-reduce.4
  209.4 30.5 reduce-scatter.1
where the time goes:
time: 249 us; the launch traced here: 248 us
  waiting for transfers between devices  123 us (49%)
  blocking collectives  77.1 us (31%)
  matrix products  22.4 us (9%)
  between operations  13.2 us (5%)
  other arithmetic  9.28 us (4%)
  local copies, waits for them, and re-layouts  2.9 us (1%)
    psum x1, waiting for transfers between devices, shards(): block_sum = lax.psum(partial_value, 'tp')  51.7 us
    all_gather x1, blocking collectives, shards(): gathered = lax.all_gather(stream, ('kv', 'tp'), axis=1, tiled=True)  44.6 us
    psum x1, waiting for transfers between devices, shards(): hidden = squared_relu(lax.psum(up_partial, 'kv'))  40.4 us
    reduce_scatter x1, waiting for transfers between devices, shards(): lax.psum_scatter(down_partial, 'tp', scatter_dimension=1, tiled=True)  30.7 us
    all_gather x3, blocking collectives, combined_all(): gathered = jax.tree.map(lambda a: lax.all_gather(a, axis), part)  22.6 us
    psum x1, blocking collectives, shards(): squares = lax.psum(row_squares(middle_block), 'kv')  9.84 us
    dot_general x1, matrix products, shards(): jnp.einsum('bhp,bhpd->bhd', weights, value_cache, preferred_element_type=...  5.65 us
  transfers between devices with their start and end apart: 3, of which 3 were waited for; matrix products, arithmetic and copies ran while one was open for 0% of the time, Pallas kernels for 0%

commit v1 on v0

--- a/solution.py
+++ b/solution.py
@@ -1,6 +1,10 @@
+import functools
+
 import jax
 import jax.numpy as jnp
 from jax import lax
+from jax.experimental import pallas as pl
+from jax.experimental.pallas import tpu as pltpu
 from jax.sharding import PartitionSpec as P
 
 D = 4096
@@ -48,7 +52,7 @@
     return jnp.sum(widened * widened, axis=1)
 
 
-def shards(
+def shards_general(
     stream,
     mixer_gain,
     query_weight,
@@ -130,9 +134,365 @@
     return (middle_piece.astype(jnp.float32) + reduced).astype(jnp.bfloat16)
 
 
+LANES = 128
+HEAD_LANES = 64
+F32 = jnp.float32
+BF16 = jnp.bfloat16
+CONTRACT_LAST = (((1,), (1,)), ((), ()))
+
+
+def iota(shape, axis):
+    return lax.broadcasted_iota(jnp.int32, shape, axis)
+
+
+def dot(one, two):
+    return jnp.dot(one, two, preferred_element_type=F32)
+
+
+def exact_dot(one, two):
+    return jnp.dot(one, two, preferred_element_type=F32, precision=lax.Precision.HIGHEST)
+
+
+def kernel_call(body, out_shapes, arguments, scratch=(), limit=8, cost=None):
+    return pl.pallas_call(
+        body,
+        out_shape=tuple(out_shapes),
+        in_specs=[pl.BlockSpec(memory_space=pltpu.VMEM)] * len(arguments),
+        out_specs=tuple(pl.BlockSpec(memory_space=pltpu.VMEM) for _ in out_shapes),
+        scratch_shapes=list(scratch),
+        cost_estimate=cost,
+        compiler_params=pltpu.CompilerParams(vmem_limit_bytes=limit << 20),
+    )(*arguments)
+
+
+def shape_of(shape, dtype):
+    return jax.ShapeDtypeStruct(shape, dtype)
+
+
+def fan_kernel(piece, copies):
+    value = piece[...]
+    for index in range(copies.shape[0]):
+        copies[index] = value
+
+
+def attention_kernel(
+    local_heads,
+    blocks,
+    gain,
+    query_weight,
+    key_weight,
+    value_weight,
+    forget_weight,
+    forget_bias,
+    keys,
+    values,
+    decay,
+    part,
+    newest,
+    normed,
+):
+    groups = keys.shape[0]
+    count, batch, _ = blocks.shape
+    rows = batch * local_heads
+    squares = jnp.zeros((batch, LANES), F32)
+    for block in range(count):
+        wide = blocks[block].astype(F32)
+        squares = squares + wide * wide
+    mean = jnp.sum(squares, axis=1, keepdims=True) / (count * LANES)
+    inverse = lax.rsqrt(mean + EPS)
+    for block in range(count):
+        scaled = blocks[block].astype(F32) * inverse * gain[block : block + 1, :]
+        normed[:, block * LANES : (block + 1) * LANES] = scaled.astype(BF16)
+    rounded = normed[...]
+    query = dot(rounded, query_weight[...]).astype(BF16)
+    logits = lax.dot_general(
+        rounded, forget_weight[...], CONTRACT_LAST, preferred_element_type=F32
+    )
+    logits = logits + forget_bias[...]
+    forget = jnp.minimum(logits, 0.0) - jnp.log1p(jnp.exp(-jnp.abs(logits)))
+    spread = (iota((rows, batch), 0) // local_heads == iota((rows, batch), 1)).astype(F32)
+    head_of_row = iota((rows, 1), 0) % local_heads
+    heads = forget.shape[1]
+    own_head = iota((rows, heads), 1) == lax.axis_index("tp") * local_heads + head_of_row
+    forget_rows = jnp.sum(
+        jnp.where(own_head, exact_dot(spread, forget), 0.0), axis=1, keepdims=True
+    )
+    spread_short = spread.astype(BF16)
+    query_rows = dot(spread_short, query)
+    depth = keys.shape[1]
+    per_group = rows // groups
+    repeats = depth // query_rows.shape[1]
+    query_wide = jnp.concatenate([query_rows] * repeats, axis=1)
+    diagonal = iota((rows, depth), 1) // HEAD_LANES == iota((rows, depth), 0) % per_group
+    query_wide = jnp.where(diagonal, query_wide, 0.0).astype(BF16)
+    diagonal = iota((per_group, depth), 1) // HEAD_LANES == iota((per_group, depth), 0)
+    lane = iota((per_group, LANES), 1)
+    scale = float(HEAD_LANES) ** (-0.5)
+    batches = batch // groups
+    for group in range(groups):
+        low = group * per_group
+        scores = dot(query_wide[low : low + per_group], keys[group]) * scale
+        fade = decay[group * batches : (group + 1) * batches].reshape(per_group, -1)
+        scores = scores + forget_rows[low : low + per_group] + fade
+        top = jnp.max(scores, axis=1, keepdims=True)
+        weights = jnp.exp(scores - top).astype(BF16)
+        total = jnp.sum(weights.astype(F32), axis=1, keepdims=True)
+        sums = lax.dot_general(
+            weights, values[group], CONTRACT_LAST, preferred_element_type=F32
+        )
+        sums = jnp.where(diagonal, sums, 0.0)
+        folded = sums[:, :LANES]
+        for low_lane in range(LANES, depth, LANES):
+            folded = folded + sums[:, low_lane : low_lane + LANES]
+        folded = folded + pltpu.roll(folded, HEAD_LANES, 1)
+        part[low : low + per_group, :] = jnp.where(
+            lane < HEAD_LANES, folded, jnp.where(lane < 96, top, total)
+        )
+    key_new = dot(rounded, key_weight[...]).astype(BF16)
+    value_new = dot(rounded, value_weight[...]).astype(BF16)
+    product = query.astype(F32) * key_new.astype(F32)
+    mine = iota((rows, LANES), 1) // HEAD_LANES == iota((rows, LANES), 0) % local_heads
+    own = jnp.sum(jnp.where(mine, exact_dot(spread, product), 0.0), axis=1, keepdims=True) * scale
+    value_rows = jnp.where(mine, dot(spread_short, value_new), 0.0)
+    value_rows = value_rows + pltpu.roll(value_rows, HEAD_LANES, 1)
+    newest[...] = jnp.where(iota((rows, LANES), 1) < HEAD_LANES, value_rows, own)
+
+
+def merge_kernel(local_heads, count, *refs):
+    parts = [ref[...] for ref in refs[:count]]
+    newest, out_weight, short, full = refs[count:]
+    rows = newest.shape[0]
+    lane = iota((rows, LANES), 1)
+
+    def pick(array, index):
+        return jnp.sum(jnp.where(lane == index, array, 0.0), axis=1, keepdims=True)
+
+    tops = [pick(array, HEAD_LANES) for array in parts]
+    totals = [pick(array, 96) for array in parts]
+    latest = newest[...]
+    own = pick(latest, HEAD_LANES)
+    peak = own
+    for top in tops:
+        peak = jnp.maximum(peak, top)
+    own_factor = jnp.exp(own - peak)
+    numer = latest * own_factor
+    denom = own_factor
+    for array, top, total in zip(parts, tops, totals):
+        factor = jnp.exp(top - peak)
+        numer = numer + array * factor
+        denom = denom + total * factor
+    ratio = jnp.where(lane < HEAD_LANES, numer / denom, 0.0)
+    ratio = ratio + pltpu.roll(ratio, HEAD_LANES, 1)
+    mine = lane // HEAD_LANES == iota((rows, LANES), 0) % local_heads
+    ratio = jnp.where(mine, ratio, 0.0).astype(BF16)
+    batch = rows // local_heads
+    gather = (iota((batch, rows), 1) // local_heads == iota((batch, rows), 0)).astype(BF16)
+    attention = dot(gather, ratio).astype(BF16)
+    product = dot(attention, out_weight[...])
+    full[...] = product
+    short[...] = product.astype(BF16)
+
+
+def add_kernel(*refs):
+    total = refs[0][...]
+    for ref in refs[1:-1]:
+        total = total + ref[...].astype(F32)
+    refs[-1][...] = total
+
+
+def up_kernel(kv, tp, one, two, blocks, gain, up_weight, short, full, piece, middle, mixed):
+    first = lax.axis_index("kv") * tp
+    total = one[...] + two[...]
+    batch = total.shape[0]
+    squares = jnp.zeros((batch, LANES), F32)
+    for block in range(tp):
+        low = block * LANES
+        value = (blocks[first + block].astype(F32) + total[:, low : low + LANES]).astype(BF16)
+        wide = value.astype(F32)
+        middle[block] = wide
+        squares = squares + wide * wide
+        mixed[:, low : low + LANES] = (wide * gain[pl.ds(first + block, 1), :]).astype(BF16)
+    piece[...] = middle[lax.axis_index("tp")]
+    product = dot(mixed[...], up_weight[...])
+    width = product.shape[1]
+    full[...] = product
+    short[:, :width] = product.astype(BF16)
+    rest = jnp.sum(squares, axis=1, keepdims=True)
+    lane = iota((batch, LANES), 1)
+    tail = jnp.zeros((batch, LANES), F32)
+    for index in range(3):
+        digit = rest.astype(BF16).astype(F32)
+        tail = jnp.where(lane == index, digit, tail)
+        rest = rest - digit
+    short[:, width:] = tail.astype(BF16)
+
+
+def down_kernel(tp, size, count, *refs):
+    full, short = refs[0], refs[1]
+    others = refs[2 : 1 + count]
+    down_weight, keep, send, shares = refs[1 + count :]
+    width = full.shape[1]
+    total = full[...]
+    tail = short[:, width:].astype(F32)
+    for ref in others:
+        total = total + ref[:, :width].astype(F32)
+        tail = tail + ref[:, width:].astype(F32)
+    mean = jnp.sum(tail, axis=1, keepdims=True) / size
+    active = jnp.maximum(total * lax.rsqrt(mean + EPS), 0.0)
+    product = dot((active * active).astype(BF16), down_weight[...])
+    for block in range(tp):
+        shares[block] = product[:, block * LANES : (block + 1) * LANES]
+    core = lax.rem(lax.axis_index("tp"), 2)
+    for pair in range(tp // 2):
+        keep[pair] = shares[2 * pair + core]
+        send[pair] = shares[2 * pair + 1 - core]
+
+
+def split_kernel(pairs, keep, other, *refs):
+    outs, own, shares = refs[:-2], refs[-2], refs[-1]
+    shares[...] = keep[...] + other[...]
+    place = lax.div(lax.axis_index("tp"), 2)
+    own[...] = shares[place]
+    for step in range(1, pairs):
+        outs[step - 1][...] = shares[lax.rem(place + step, pairs)].astype(BF16)
+
+
+def last_kernel(*refs):
+    total = refs[0][...]
+    for ref in refs[1:-1]:
+        total = total + ref[...].astype(F32)
+    refs[-1][...] = total.astype(BF16)
+
+
+def shards(
+    kv,
+    tp,
+    stream,
+    mixer_gain,
+    query_weight,
+    key_weight,
+    value_weight,
+    forget_weight,
+    forget_bias,
+    key_cache,
+    value_cache,
+    past_decay,
+    out_weight,
+    channel_gain,
+    up_weight,
+    down_weight,
+):
+    batch, piece_width = stream.shape
+    _, local_heads, places, head_size = key_cache.shape
+    rows = batch * local_heads
+    fits = (
+        piece_width == LANES
+        and head_size == HEAD_LANES
+        and local_heads == LANES // HEAD_LANES
+        and tp % 2 == 0
+        and rows % 8 == 0
+        and places % LANES == 0
+        and out_weight.shape[1] == tp * LANES
+    )
+    if not fits:
+        return shards_general(
+            stream,
+            mixer_gain,
+            query_weight,
+            key_weight,
+            value_weight,
+            forget_weight,
+            forget_bias,
+            key_cache,
+            value_cache,
+            past_decay,
+            out_weight,
+            channel_gain,
+            up_weight,
+            down_weight,
+        )
+    count = kv * tp
+    size = count * piece_width
+    groups = rows // 8
+    depth = 8 * head_size
+    (fanned,) = kernel_call(
+        fan_kernel,
+        [shape_of((count, batch, piece_width), BF16)],
+        (stream,),
+        cost=pl.CostEstimate(flops=40_000_000_000, bytes_accessed=0, transcendentals=0),
+    )
+    blocks = lax.all_to_all(fanned, ("kv", "tp"), 0, 0)
+    keys = jnp.swapaxes(key_cache, 2, 3).reshape(groups, depth, places)
+    values = jnp.swapaxes(value_cache, 2, 3).reshape(groups, depth, places)
+    heads = forget_bias.shape[0]
+    part, newest = kernel_call(
+        functools.partial(attention_kernel, local_heads),
+        [shape_of((rows, LANES), F32)] * 2,
+        (
+            blocks,
+            mixer_gain.reshape(count, LANES),
+            query_weight,
+            key_weight,
+            value_weight,
+            forget_weight.T,
+            forget_bias.reshape(1, heads),
+            keys,
+            values,
+            past_decay,
+        ),
+        scratch=[pltpu.VMEM((batch, size), BF16)],
+    )
+    def turn(array, axis, length, step, stride=1):
+        total = length * stride
+        return lax.ppermute(array, axis, [(i, (i + step * stride) % total) for i in range(total)])
+
+    def swap(array):
+        return lax.ppermute(array, "tp", [(i, i ^ 1) for i in range(tp)])
+
+    pairs = tp // 2
+    others = [turn(part, "kv", kv, step) for step in range(1, kv)]
+    block_width = out_weight.shape[1]
+    short, full = kernel_call(
+        functools.partial(merge_kernel, local_heads, kv),
+        [shape_of((batch, block_width), BF16), shape_of((batch, block_width), F32)],
+        (part, *others, newest, out_weight),
+    )
+    others = [turn(short, "tp", pairs, step, 2) for step in range(1, pairs)]
+    (column_sum,) = kernel_call(add_kernel, [shape_of((batch, block_width), F32)], (full, *others))
+    width = up_weight.shape[1]
+    short, full, piece = kernel_call(
+        functools.partial(up_kernel, kv, tp),
+        [
+            shape_of((batch, width + LANES), BF16),
+            shape_of((batch, width), F32),
+            shape_of((batch, LANES), F32),
+        ],
+        (column_sum, swap(column_sum), blocks, channel_gain.reshape(count, LANES), up_weight),
+        scratch=[pltpu.VMEM((tp, batch, LANES), F32), pltpu.VMEM((batch, block_width), BF16)],
+    )
+    others = [turn(short, "kv", kv, step) for step in range(1, kv)]
+    keep, send = kernel_call(
+        functools.partial(down_kernel, tp, size, kv),
+        [shape_of((pairs, batch, LANES), F32)] * 2,
+        (full, short, *others, down_weight),
+        scratch=[pltpu.VMEM((tp, batch, LANES), F32)],
+    )
+    *shares, own = kernel_call(
+        functools.partial(split_kernel, pairs),
+        [shape_of((batch, LANES), BF16)] * (pairs - 1) + [shape_of((batch, LANES), F32)],
+        (keep, swap(send)),
+        scratch=[pltpu.VMEM((pairs, batch, LANES), F32)],
+    )
+    others = [turn(shares[step - 1], "tp", pairs, step, 2) for step in range(1, pairs)]
+    (updated,) = kernel_call(
+        last_kernel, [shape_of((batch, LANES), BF16)], (piece, own, *others)
+    )
+    return updated
+
+
 def solution(mesh):
     return jax.shard_map(
-        shards,
+        functools.partial(shards, mesh.shape["kv"], mesh.shape["tp"]),
         mesh=mesh,
         in_specs=(
             P(None, ("kv", "tp")),

time: 249 us -> 60.5 us (0.24)
  waiting for transfers between devices: 123 us -> 20.1 us
  blocking collectives: 77.1 us -> 17.1 us
  matrix products: 22.4 us -> 0 us
  starting transfers between devices: 0.09 us -> 13.3 us
  between operations: 13.2 us -> 0.2 us
  other arithmetic: 9.28 us -> 0 us
  Pallas kernels: 0 us -> 8.68 us
    psum x2 -> x0, waiting for transfers between devices: 92.1 us -> none  [the longest x1 51.7 us: shards(): block_sum = lax.psum(partial_value, 'tp')]
    all_gather x4 -> x0, blocking collectives: 67.2 us -> none  [the longest x1 44.6 us: shards(): gathered = lax.all_gather(stream, ('kv', 'tp'), axis=1, tiled=True)]
    reduce_scatter x1 -> x0, waiting for transfers between devices: 30.7 us -> none  [shards(): lax.psum_scatter(down_partial, 'tp', scatter_dimension=1, tiled=True)]
    dot_general x9 -> x0, matrix products: 22.4 us -> none  [the longest x1 5.65 us: shards(): jnp.einsum('bhp,bhpd->bhd', weights, value_cache, preferred_element_type=...]
    ppermute x0 -> x14, waiting for transfers between devices: none -> 20.1 us  [the longest x12 17.6 us: turn(): lax.ppermute(array, axis, [(i, (i + step * stride) % total) for i in rang...]
    all_to_all x0 -> x1, blocking collectives: none -> 17.1 us  [shards(): blocks = lax.all_to_all(fanned, ('kv', 'tp'), 0, 0)]
    ppermute x0 -> x14, starting transfers between devices: none -> 13.3 us  [the longest x12 13.1 us: turn(): lax.ppermute(array, axis, [(i, (i + step * stride) % total) for i in rang...]
    psum x1 -> x0, blocking collectives: 9.84 us -> none  [shards(): squares = lax.psum(row_squares(middle_block), 'kv')]
  transfers between devices with their start and end apart: 3 -> 14, of which waited for: 3 -> 11; matrix products, arithmetic and copies ran while one was open for 0% -> 0% of each run, Pallas kernels for 0% -> 0%
where the time goes in v1:
time: 60.5 us; the launch traced here: 60.3 us
  waiting for transfers between devices  20.1 us (33%)
  blocking collectives  17.1 us (28%)
  starting transfers between devices  13.3 us (22%)
  Pallas kernels  8.68 us (14%)
  local copies, waits for them, and re-layouts  0.9 us (1%)
    ppermute x12, waiting for transfers between devices, turn(): lax.ppermute(array, axis, [(i, (i + step * stride) % total) for i in rang...  17.6 us
    all_to_all x1, blocking collectives, shards(): blocks = lax.all_to_all(fanned, ('kv', 'tp'), 0, 0)  17.1 us
    ppermute x12, starting transfers between devices, turn(): lax.ppermute(array, axis, [(i, (i + step * stride) % total) for i in rang...  13.1 us
    pallas_call x8, Pallas kernels, kernel_call(): pl.pallas_call(body, out_shape=tuple(out_shapes), in_specs=[pl.BlockSpec(...  8.68 us
    ppermute x2, waiting for transfers between devices, swap(): return lax.ppermute(array, 'tp', [(i, i ^ 1) for i in range(tp)])  2.58 us
  transfers between devices with their start and end apart: 14, of which 11 were waited for; matrix products, arithmetic and copies ran while one was open for 0% of the time, Pallas kernels for 0%

profile of v1, /device:TPU:0, one launch (start us, length us, event | category | flops | bytes accessed | tf_op | source)
XLA Modules:
  0.0 60.3 jit_solution(15378414615566268626)
XLA Ops:
  0.1 0.8 %copy-done.13 = bf16[32,128]{1,0:T(8,128)(2,1)S(1)} copy-done((bf16[32,128]{1,0:T(8,128)(2,1)S(1)}, bf16[32,128]{1,0:T(8,128)(2,1)}, u32[]{:S(2)}) %copy-start.13) | copy-done | bytes 8216
  0.9 17.1 %all_to_all.5.blocks = bf16[32,32,128]{2,1,0:T(8,128)(2,1)S(1)} all-to-all(bf16[32,32,128]{2,1,0:T(8,128)(2,1)S(1)} %shard_map.136), channel_id=1, replica_groups=mesh['kv'=4,'tp'=8] {'kv','tp'}, dimensions={0} | all-to-all | bytes 524288 | tf_op jit(solution)/shard_map/all_to_all | solution.py:424
  18.2 5.8 %shard_map.137 = (f32[64,128]{1,0:T(8,128)S(1)}, f32[64,128]{1,0:T(8,128)S(1)}) custom-call(bf16[32,32,128]{2,1,0:T(8,128)(2,1)S(1)} %all_to_all.5.blocks, f32[32,128]{1,0:T(8,128)S(1)} %bitcast.13, bf16[4096,128]{1,0:T(8,128)(2,1)S(1)} %copy-done.4, bf16[4096,128]{1,0:T(8,128)(2,1)S(1)} %copy-done.5, bf16[4096,128]{1,0:T(8,128)(2,1)S(1)} %copy-done.6, ...), custom_call_target="tpu_custom_call" | custom-call | tf_op jit(solution)/shard_map/pallas_call | solution.py:157
  24.0 1.2 %collective-permute-start.2 = (f32[64,128]{1,0:T(8,128)S(1)}, f32[64,128]{1,0:T(8,128)S(1)}, u32[]{:S(2)}, u32[]{:S(2)}) collective-permute-start(f32[64,128]{1,0:T(8,128)S(1)} %get-tuple-element.18.refs_0_), channel_id=1, source_target_pairs={{0,24},{8,0},{16,8},{24,16},{1,25},{9,1},{17,9},{25,17},{2,26},{10... | collective-permute-start | bytes 98312 | tf_op jit(solution)/shard_map/ppermute | solution.py:447
  25.2 1.2 %collective-permute-start.1 = (f32[64,128]{1,0:T(8,128)S(1)}, f32[64,128]{1,0:T(8,128)S(1)}, u32[]{:S(2)}, u32[]{:S(2)}) collective-permute-start(f32[64,128]{1,0:T(8,128)S(1)} %get-tuple-element.18.refs_0_), channel_id=1, source_target_pairs={{0,16},{8,24},{16,0},{24,8},{1,17},{9,25},{17,1},{25,9},{2,18},{10... | collective-permute-start | bytes 98312 | tf_op jit(solution)/shard_map/ppermute | solution.py:447
  26.9 1.1 %collective-permute-done.2.refs_3_ = f32[64,128]{1,0:T(8,128)S(1)} collective-permute-done((f32[64,128]{1,0:T(8,128)S(1)}, f32[64,128]{1,0:T(8,128)S(1)}, u32[]{:S(2)}, u32[]{:S(2)}) %collective-permute-start.2) | collective-permute-done | bytes 32800 | tf_op jit(solution)/shard_map/ppermute | solution.py:447
  28.1 1.0 %collective-permute-done.1.refs_2_ = f32[64,128]{1,0:T(8,128)S(1)} collective-permute-done((f32[64,128]{1,0:T(8,128)S(1)}, f32[64,128]{1,0:T(8,128)S(1)}, u32[]{:S(2)}, u32[]{:S(2)}) %collective-permute-start.1) | collective-permute-done | bytes 32800 | tf_op jit(solution)/shard_map/ppermute | solution.py:447
  29.1 2.1 %collective-permute-done.refs_1_ = f32[64,128]{1,0:T(8,128)S(1)} collective-permute-done((f32[64,128]{1,0:T(8,128)S(1)}, f32[64,128]{1,0:T(8,128)S(1)}, u32[]{:S(2)}, u32[]{:S(2)}) %collective-permute-start) | collective-permute-done | bytes 32800 | tf_op jit(solution)/shard_map/ppermute | solution.py:447
  31.6 1.4 %collective-permute-start.5 = (bf16[32,1024]{1,0:T(8,128)(2,1)S(1)}, bf16[32,1024]{1,0:T(8,128)(2,1)S(1)}, u32[]{:S(2)}, u32[]{:S(2)}) collective-permute-start(bf16[32,1024]{1,0:T(8,128)(2,1)S(1)} %get-tuple-element.21), channel_id=1, source_target_pairs={{0,6},{1,7},{2,0},{3,1},{4,2},{5,3},{6,4},{7,5},{8,14},{9,15},{10,... | collective-permute-start | bytes 196616 | tf_op jit(solution)/shard_map/ppermute | solution.py:447
  33.0 1.9 %collective-permute-start.3 = (bf16[32,1024]{1,0:T(8,128)(2,1)S(1)}, bf16[32,1024]{1,0:T(8,128)(2,1)S(1)}, u32[]{:S(2)}, u32[]{:S(2)}) collective-permute-start(bf16[32,1024]{1,0:T(8,128)(2,1)S(1)} %get-tuple-element.21), channel_id=1, source_target_pairs={{0,2},{1,3},{2,4},{3,5},{4,6},{5,7},{6,0},{7,1},{8,10},{9,11},{10,... | collective-permute-start | bytes 196616 | tf_op jit(solution)/shard_map/ppermute | solution.py:447
  34.9 1.4 %collective-permute-done.5.refs_3_ = bf16[32,1024]{1,0:T(8,128)(2,1)S(1)} collective-permute-done((bf16[32,1024]{1,0:T(8,128)(2,1)S(1)}, bf16[32,1024]{1,0:T(8,128)(2,1)S(1)}, u32[]{:S(2)}, u32[]{:S(2)}) %collective-permute-start.5) | collective-permute-done | bytes 65568 | tf_op jit(solution)/shard_map/ppermute | solution.py:447
  36.3 3.3 %collective-permute-done.4.refs_2_ = bf16[32,1024]{1,0:T(8,128)(2,1)S(1)} collective-permute-done((bf16[32,1024]{1,0:T(8,128)(2,1)S(1)}, bf16[32,1024]{1,0:T(8,128)(2,1)S(1)}, u32[]{:S(2)}, u32[]{:S(2)}) %collective-permute-start.4) | collective-permute-done | bytes 65568 | tf_op jit(solution)/shard_map/ppermute | solution.py:447
  39.7 1.3 %collective-permute-done.6.two = f32[32,1024]{1,0:T(8,128)S(1)} collective-permute-done((f32[32,1024]{1,0:T(8,128)S(1)}, f32[32,1024]{1,0:T(8,128)S(1)}, u32[]{:S(2)}, u32[]{:S(2)}) %collective-permute-start.6) | collective-permute-done | bytes 131104 | tf_op jit(solution)/shard_map/ppermute | solution.py:450
  41.0 0.8 %shard_map.140 = (bf16[32,2176]{1,0:T(8,128)(2,1)S(1)}, f32[32,2048]{1,0:T(8,128)S(1)}, f32[32,128]{1,0:T(8,128)S(1)}) custom-call(f32[32,1024]{1,0:T(8,128)S(1)} %shard_map.139.one, f32[32,1024]{1,0:T(8,128)S(1)} %collective-permute-done.6.two, bf16[32,32,128]{2,1,0:T(8,128)(2,1)S(1)} %all_to_all.5.blocks, f32[32,128]{1,0:T(8,128)S(1)} %bitcast.14, ...), custom_call_target="tpu_custom_call" | custom-call | tf_op jit(solution)/shard_map/pallas_call | solution.py:157
  41.9 1.1 %collective-permute-start.9 = (bf16[32,2176]{1,0:T(8,128)(2,1)S(1)}, bf16[32,2176]{1,0:T(8,128)(2,1)S(1)}, u32[]{:S(2)}, u32[]{:S(2)}) collective-permute-start(bf16[32,2176]{1,0:T(8,128)(2,1)S(1)} %get-tuple-element.24.refs_1_), channel_id=1, source_target_pairs={{0,24},{8,0},{16,8},{24,16},{1,25},{9,1},{17,9},{25,17},{2,26},{10... | collective-permute-start | bytes 417800 | tf_op jit(solution)/shard_map/ppermute | solution.py:447
  43.5 1.4 %collective-permute-start.7 = (bf16[32,2176]{1,0:T(8,128)(2,1)S(1)}, bf16[32,2176]{1,0:T(8,128)(2,1)S(1)}, u32[]{:S(2)}, u32[]{:S(2)}) collective-permute-start(bf16[32,2176]{1,0:T(8,128)(2,1)S(1)} %get-tuple-element.24.refs_1_), channel_id=1, source_target_pairs={{0,8},{8,16},{16,24},{24,0},{1,9},{9,17},{17,25},{25,1},{2,10},{10... | collective-permute-start | bytes 417800 | tf_op jit(solution)/shard_map/ppermute | solution.py:447
  44.9 3.5 %collective-permute-done.9.refs_4_ = bf16[32,2176]{1,0:T(8,128)(2,1)S(1)} collective-permute-done((bf16[32,2176]{1,0:T(8,128)(2,1)S(1)}, bf16[32,2176]{1,0:T(8,128)(2,1)S(1)}, u32[]{:S(2)}, u32[]{:S(2)}) %collective-permute-start.9) | collective-permute-done | bytes 139296 | tf_op jit(solution)/shard_map/ppermute | solution.py:447
  48.4 2.9 %collective-permute-done.8.refs_3_ = bf16[32,2176]{1,0:T(8,128)(2,1)S(1)} collective-permute-done((bf16[32,2176]{1,0:T(8,128)(2,1)S(1)}, bf16[32,2176]{1,0:T(8,128)(2,1)S(1)}, u32[]{:S(2)}, u32[]{:S(2)}) %collective-permute-start.8) | collective-permute-done | bytes 139296 | tf_op jit(solution)/shard_map/ppermute | solution.py:447
  51.4 0.9 %shard_map.141 = (f32[4,32,128]{2,1,0:T(8,128)S(1)}, f32[4,32,128]{2,1,0:T(8,128)S(1)}) custom-call(f32[32,2048]{1,0:T(8,128)S(1)} %get-tuple-element.23.refs_0_, bf16[32,2176]{1,0:T(8,128)(2,1)S(1)} %get-tuple-element.24.refs_1_, bf16[32,2176]{1,0:T(8,128)(2,1)S(1)} %collective-permute-done.7.refs_2_, bf16[32,2176]{1,0:T(8,128)(2,1)S(1)} %collective-permute-done.8.refs_3_, ...), custom_call_target="tpu_custom_call" | custom-call | tf_op jit(solution)/shard_map/pallas_call | solution.py:157
  52.4 1.2 %collective-permute-done.10.other = f32[4,32,128]{2,1,0:T(8,128)S(1)} collective-permute-done((f32[4,32,128]{2,1,0:T(8,128)S(1)}, f32[4,32,128]{2,1,0:T(8,128)S(1)}, u32[]{:S(2)}, u32[]{:S(2)}) %collective-permute-start.10) | collective-permute-done | bytes 65568 | tf_op jit(solution)/shard_map/ppermute | solution.py:450
  53.7 1.3 %collective-permute-start.12 = (bf16[32,128]{1,0:T(8,128)(2,1)S(1)}, bf16[32,128]{1,0:T(8,128)(2,1)S(1)}, u32[]{:S(2)}, u32[]{:S(2)}) collective-permute-start(bf16[32,128]{1,0:T(8,128)(2,1)S(1)} %get-tuple-element.29), channel_id=1, source_target_pairs={{0,4},{1,5},{2,6},{3,7},{4,0},{5,1},{6,2},{7,3},{8,12},{9,13},{10,... | collective-permute-start | bytes 24584 | tf_op jit(solution)/shard_map/ppermute | solution.py:447
  55.0 2.5 %collective-permute-start.13 = (bf16[32,128]{1,0:T(8,128)(2,1)S(1)}, bf16[32,128]{1,0:T(8,128)(2,1)S(1)}, u32[]{:S(2)}, u32[]{:S(2)}) collective-permute-start(bf16[32,128]{1,0:T(8,128)(2,1)S(1)} %get-tuple-element.30), channel_id=1, source_target_pairs={{0,6},{1,7},{2,0},{3,1},{4,2},{5,3},{6,4},{7,5},{8,14},{9,15},{10,... | collective-permute-start | bytes 24584 | tf_op jit(solution)/shard_map/ppermute | solution.py:447
  57.5 1.6 %collective-permute-done.11.refs_2_ = bf16[32,128]{1,0:T(8,128)(2,1)S(1)} collective-permute-done((bf16[32,128]{1,0:T(8,128)(2,1)S(1)}, bf16[32,128]{1,0:T(8,128)(2,1)S(1)}, u32[]{:S(2)}, u32[]{:S(2)}) %collective-permute-start.11) | collective-permute-done | bytes 8224 | tf_op jit(solution)/shard_map/ppermute | solution.py:447
  59.7 0.6 %shard_map.143 = bf16[32,128]{1,0:T(8,128)(2,1)} custom-call(f32[32,128]{1,0:T(8,128)S(1)} %get-tuple-element.22.refs_0_, f32[32,128]{1,0:T(8,128)S(1)} %get-tuple-element.27.refs_1_, bf16[32,128]{1,0:T(8,128)(2,1)S(1)} %collective-permute-done.11.refs_2_, bf16[32,128]{1,0:T(8,128)(2,1)S(1)} %collective-permute-done.12.refs_3_, ...), custom_call_target="tpu_custom_call" | custom-call | tf_op jit(solution)/shard_map/pallas_call | solution.py:157
  (41 shorter events, 2.5 us)
Async XLA Ops:
  0.0 18.1 %copy-start = (bf16[32,2,1024,64]{2,3,1,0:T(8,128)(2,1)S(1)}, bf16[32,2,1024,64]{2,3,1,0:T(8,128)(2,1)}, u32[]{:S(2)}) copy-start(bf16[32,2,1024,64]{2,3,1,0:T(8,128)(2,1)} %param.21) | copy-start | bytes 25165828
  0.0 18.1 %copy-start.12 = (f32[16]{0:T(128)S(1)}, f32[16]{0:T(128)}, u32[]{:S(2)}) copy-start(f32[16]{0:T(128)} %param.20) | copy-start | bytes 196
  0.0 18.1 %copy-start.9 = (bf16[4096,16]{0,1:T(8,128)(2,1)S(1)}, bf16[4096,16]{0,1:T(8,128)(2,1)}, u32[]{:S(2)}) copy-start(bf16[4096,16]{0,1:T(8,128)(2,1)} %param.19) | copy-start | bytes 393220
  0.0 18.1 %copy-start.6 = (bf16[4096,128]{1,0:T(8,128)(2,1)S(1)}, bf16[4096,128]{1,0:T(8,128)(2,1)}, u32[]{:S(2)}) copy-start(bf16[4096,128]{1,0:T(8,128)(2,1)} %value_weight.1) | copy-start | bytes 3145732
  0.0 18.1 %copy-start.5 = (bf16[4096,128]{1,0:T(8,128)(2,1)S(1)}, bf16[4096,128]{1,0:T(8,128)(2,1)}, u32[]{:S(2)}) copy-start(bf16[4096,128]{1,0:T(8,128)(2,1)} %key_weight.1) | copy-start | bytes 3145732
  0.0 18.1 %copy-start.4 = (bf16[4096,128]{1,0:T(8,128)(2,1)S(1)}, bf16[4096,128]{1,0:T(8,128)(2,1)}, u32[]{:S(2)}) copy-start(bf16[4096,128]{1,0:T(8,128)(2,1)} %query_weight.1) | copy-start | bytes 3145732
  0.0 18.1 %copy-start.10 = (f32[4096]{0:T(1024)S(1)}, f32[4096]{0:T(1024)}, u32[]{:S(2)}) copy-start(f32[4096]{0:T(1024)} %param.15) | copy-start | bytes 49156
  18.2 22.9 %copy-start.2 = (bf16[1024,2048]{1,0:T(8,128)(2,1)S(1)}, bf16[1024,2048]{1,0:T(8,128)(2,1)}, u32[]{:S(2)}) copy-start(bf16[1024,2048]{1,0:T(8,128)(2,1)} %up_weight.1) | copy-start | bytes 12582916
  18.2 22.9 %copy-start.11 = (f32[4096]{0:T(1024)S(1)}, f32[4096]{0:T(1024)}, u32[]{:S(2)}) copy-start(f32[4096]{0:T(1024)} %param.25) | copy-start | bytes 49156
  18.2 33.2 %copy-start.3 = (bf16[2048,1024]{1,0:T(8,128)(2,1)S(1)}, bf16[2048,1024]{1,0:T(8,128)(2,1)}, u32[]{:S(2)}) copy-start(bf16[2048,1024]{1,0:T(8,128)(2,1)} %refs_5_.3) | copy-start | bytes 12582916
  24.0 4.1 %collective-permute-start.2 = (f32[64,128]{1,0:T(8,128)S(1)}, f32[64,128]{1,0:T(8,128)S(1)}, u32[]{:S(2)}, u32[]{:S(2)}) collective-permute-start(f32[64,128]{1,0:T(8,128)S(1)} %get-tuple-element.18.refs_0_), channel_id=1, source_target_pairs={{0,24},{8,0},{16,8},{24,16},{1,25},{9,1},{17,9},{25,17},{2,26},{10... | collective-permute-start | bytes 98312 | tf_op jit(solution)/shard_map/ppermute | solution.py:447
  25.2 3.9 %collective-permute-start.1 = (f32[64,128]{1,0:T(8,128)S(1)}, f32[64,128]{1,0:T(8,128)S(1)}, u32[]{:S(2)}, u32[]{:S(2)}) collective-permute-start(f32[64,128]{1,0:T(8,128)S(1)} %get-tuple-element.18.refs_0_), channel_id=1, source_target_pairs={{0,16},{8,24},{16,0},{24,8},{1,17},{9,25},{17,1},{25,9},{2,18},{10... | collective-permute-start | bytes 98312 | tf_op jit(solution)/shard_map/ppermute | solution.py:447
  26.4 4.8 %collective-permute-start = (f32[64,128]{1,0:T(8,128)S(1)}, f32[64,128]{1,0:T(8,128)S(1)}, u32[]{:S(2)}, u32[]{:S(2)}) collective-permute-start(f32[64,128]{1,0:T(8,128)S(1)} %get-tuple-element.18.refs_0_), channel_id=1, source_target_pairs={{0,8},{8,16},{16,24},{24,0},{1,9},{9,17},{17,25},{25,1},{2,10},{10... | collective-permute-start | bytes 98312 | tf_op jit(solution)/shard_map/ppermute | solution.py:447
  31.6 4.7 %collective-permute-start.5 = (bf16[32,1024]{1,0:T(8,128)(2,1)S(1)}, bf16[32,1024]{1,0:T(8,128)(2,1)S(1)}, u32[]{:S(2)}, u32[]{:S(2)}) collective-permute-start(bf16[32,1024]{1,0:T(8,128)(2,1)S(1)} %get-tuple-element.21), channel_id=1, source_target_pairs={{0,6},{1,7},{2,0},{3,1},{4,2},{5,3},{6,4},{7,5},{8,14},{9,15},{10,... | collective-permute-start | bytes 196616 | tf_op jit(solution)/shard_map/ppermute | solution.py:447
  33.0 6.6 %collective-permute-start.4 = (bf16[32,1024]{1,0:T(8,128)(2,1)S(1)}, bf16[32,1024]{1,0:T(8,128)(2,1)S(1)}, u32[]{:S(2)}, u32[]{:S(2)}) collective-permute-start(bf16[32,1024]{1,0:T(8,128)(2,1)S(1)} %get-tuple-element.21), channel_id=1, source_target_pairs={{0,4},{1,5},{2,6},{3,7},{4,0},{5,1},{6,2},{7,3},{8,12},{9,13},{10,... | collective-permute-start | bytes 196616 | tf_op jit(solution)/shard_map/ppermute | solution.py:447
  33.0 6.6 %collective-permute-start.3 = (bf16[32,1024]{1,0:T(8,128)(2,1)S(1)}, bf16[32,1024]{1,0:T(8,128)(2,1)S(1)}, u32[]{:S(2)}, u32[]{:S(2)}) collective-permute-start(bf16[32,1024]{1,0:T(8,128)(2,1)S(1)} %get-tuple-element.21), channel_id=1, source_target_pairs={{0,2},{1,3},{2,4},{3,5},{4,6},{5,7},{6,0},{7,1},{8,10},{9,11},{10,... | collective-permute-start | bytes 196616 | tf_op jit(solution)/shard_map/ppermute | solution.py:447
  39.6 1.4 %collective-permute-start.6 = (f32[32,1024]{1,0:T(8,128)S(1)}, f32[32,1024]{1,0:T(8,128)S(1)}, u32[]{:S(2)}, u32[]{:S(2)}) collective-permute-start(f32[32,1024]{1,0:T(8,128)S(1)} %shard_map.139.one), channel_id=1, source_target_pairs={{0,1},{1,0},{2,3},{3,2},{4,5},{5,4},{6,7},{7,6},{8,9},{9,8},{10,11... | collective-permute-start | bytes 393224 | tf_op jit(solution)/shard_map/ppermute | solution.py:450
  41.9 6.6 %collective-permute-start.9 = (bf16[32,2176]{1,0:T(8,128)(2,1)S(1)}, bf16[32,2176]{1,0:T(8,128)(2,1)S(1)}, u32[]{:S(2)}, u32[]{:S(2)}) collective-permute-start(bf16[32,2176]{1,0:T(8,128)(2,1)S(1)} %get-tuple-element.24.refs_1_), channel_id=1, source_target_pairs={{0,24},{8,0},{16,8},{24,16},{1,25},{9,1},{17,9},{25,17},{2,26},{10... | collective-permute-start | bytes 417800 | tf_op jit(solution)/shard_map/ppermute | solution.py:447
  42.9 8.4 %collective-permute-start.8 = (bf16[32,2176]{1,0:T(8,128)(2,1)S(1)}, bf16[32,2176]{1,0:T(8,128)(2,1)S(1)}, u32[]{:S(2)}, u32[]{:S(2)}) collective-permute-start(bf16[32,2176]{1,0:T(8,128)(2,1)S(1)} %get-tuple-element.24.refs_1_), channel_id=1, source_target_pairs={{0,16},{8,24},{16,0},{24,8},{1,17},{9,25},{17,1},{25,9},{2,18},{10... | collective-permute-start | bytes 417800 | tf_op jit(solution)/shard_map/ppermute | solution.py:447
  43.5 7.9 %collective-permute-start.7 = (bf16[32,2176]{1,0:T(8,128)(2,1)S(1)}, bf16[32,2176]{1,0:T(8,128)(2,1)S(1)}, u32[]{:S(2)}, u32[]{:S(2)}) collective-permute-start(bf16[32,2176]{1,0:T(8,128)(2,1)S(1)} %get-tuple-element.24.refs_1_), channel_id=1, source_target_pairs={{0,8},{8,16},{16,24},{24,0},{1,9},{9,17},{17,25},{25,1},{2,10},{10... | collective-permute-start | bytes 417800 | tf_op jit(solution)/shard_map/ppermute | solution.py:447
  52.3 1.3 %collective-permute-start.10 = (f32[4,32,128]{2,1,0:T(8,128)S(1)}, f32[4,32,128]{2,1,0:T(8,128)S(1)}, u32[]{:S(2)}, u32[]{:S(2)}) collective-permute-start(f32[4,32,128]{2,1,0:T(8,128)S(1)} %get-tuple-element.26), channel_id=1, source_target_pairs={{0,1},{1,0},{2,3},{3,2},{4,5},{5,4},{6,7},{7,6},{8,9},{9,8},{10,11... | collective-permute-start | bytes 196616 | tf_op jit(solution)/shard_map/ppermute | solution.py:450
  53.6 5.5 %collective-permute-start.11 = (bf16[32,128]{1,0:T(8,128)(2,1)S(1)}, bf16[32,128]{1,0:T(8,128)(2,1)S(1)}, u32[]{:S(2)}, u32[]{:S(2)}) collective-permute-start(bf16[32,128]{1,0:T(8,128)(2,1)S(1)} %get-tuple-element.28), channel_id=1, source_target_pairs={{0,2},{1,3},{2,4},{3,5},{4,6},{5,7},{6,0},{7,1},{8,10},{9,11},{10,... | collective-permute-start | bytes 24584 | tf_op jit(solution)/shard_map/ppermute | solution.py:447
  53.7 5.4 %collective-permute-start.12 = (bf16[32,128]{1,0:T(8,128)(2,1)S(1)}, bf16[32,128]{1,0:T(8,128)(2,1)S(1)}, u32[]{:S(2)}, u32[]{:S(2)}) collective-permute-start(bf16[32,128]{1,0:T(8,128)(2,1)S(1)} %get-tuple-element.29), channel_id=1, source_target_pairs={{0,4},{1,5},{2,6},{3,7},{4,0},{5,1},{6,2},{7,3},{8,12},{9,13},{10,... | collective-permute-start | bytes 24584 | tf_op jit(solution)/shard_map/ppermute | solution.py:447
  55.0 4.7 %collective-permute-start.13 = (bf16[32,128]{1,0:T(8,128)(2,1)S(1)}, bf16[32,128]{1,0:T(8,128)(2,1)S(1)}, u32[]{:S(2)}, u32[]{:S(2)}) collective-permute-start(bf16[32,128]{1,0:T(8,128)(2,1)S(1)} %get-tuple-element.30), channel_id=1, source_target_pairs={{0,6},{1,7},{2,0},{3,1},{4,2},{5,3},{6,4},{7,5},{8,14},{9,15},{10,... | collective-permute-start | bytes 24584 | tf_op jit(solution)/shard_map/ppermute | solution.py:447
  (4 other events, 50.0 us)

commit v2 on v1

--- a/solution.py
+++ b/solution.py
@@ -136,6 +136,7 @@
 
 LANES = 128
 HEAD_LANES = 64
+PACK = 16
 F32 = jnp.float32
 BF16 = jnp.bfloat16
 CONTRACT_LAST = (((1,), (1,)), ((), ()))
@@ -147,10 +148,6 @@
 
 def dot(one, two):
     return jnp.dot(one, two, preferred_element_type=F32)
-
-
-def exact_dot(one, two):
-    return jnp.dot(one, two, preferred_element_type=F32, precision=lax.Precision.HIGHEST)
 
 
 def kernel_call(body, out_shapes, arguments, scratch=(), limit=8, cost=None):
@@ -180,20 +177,17 @@
     blocks,
     gain,
     query_weight,
-    key_weight,
-    value_weight,
     forget_weight,
     forget_bias,
     keys,
     values,
     decay,
     part,
-    newest,
     normed,
+    queries,
 ):
-    groups = keys.shape[0]
+    groups, depth, _ = keys.shape
     count, batch, _ = blocks.shape
-    rows = batch * local_heads
     squares = jnp.zeros((batch, LANES), F32)
     for block in range(count):
         wide = blocks[block].astype(F32)
@@ -205,90 +199,104 @@
         normed[:, block * LANES : (block + 1) * LANES] = scaled.astype(BF16)
     rounded = normed[...]
     query = dot(rounded, query_weight[...]).astype(BF16)
+    queries[...] = query
+    query = query.astype(F32)
     logits = lax.dot_general(
         rounded, forget_weight[...], CONTRACT_LAST, preferred_element_type=F32
     )
     logits = logits + forget_bias[...]
     forget = jnp.minimum(logits, 0.0) - jnp.log1p(jnp.exp(-jnp.abs(logits)))
-    spread = (iota((rows, batch), 0) // local_heads == iota((rows, batch), 1)).astype(F32)
-    head_of_row = iota((rows, 1), 0) % local_heads
-    heads = forget.shape[1]
-    own_head = iota((rows, heads), 1) == lax.axis_index("tp") * local_heads + head_of_row
-    forget_rows = jnp.sum(
-        jnp.where(own_head, exact_dot(spread, forget), 0.0), axis=1, keepdims=True
-    )
-    spread_short = spread.astype(BF16)
-    query_rows = dot(spread_short, query)
-    depth = keys.shape[1]
-    per_group = rows // groups
-    repeats = depth // query_rows.shape[1]
-    query_wide = jnp.concatenate([query_rows] * repeats, axis=1)
-    diagonal = iota((rows, depth), 1) // HEAD_LANES == iota((rows, depth), 0) % per_group
-    query_wide = jnp.where(diagonal, query_wide, 0.0).astype(BF16)
-    diagonal = iota((per_group, depth), 1) // HEAD_LANES == iota((per_group, depth), 0)
-    lane = iota((per_group, LANES), 1)
+    first_head = lax.axis_index("tp") * local_heads
+    head = iota(forget.shape, 1)
+    forgets = [
+        jnp.sum(jnp.where(head == first_head + index, forget, 0.0), axis=1, keepdims=True)
+        for index in range(local_heads)
+    ]
+    per_group = batch * local_heads // groups
+    batches = batch // groups
+    place_of = [(row // local_heads, row % local_heads) for row in range(per_group)]
+    tile_lane = iota((per_group, LANES), 1)
+    tile_row = iota((per_group, LANES), 0)
+    column = iota((HEAD_LANES, LANES), 1)
+    columns = jnp.zeros((HEAD_LANES, LANES), F32)
+    stats = jnp.zeros((per_group, LANES), F32)
     scale = float(HEAD_LANES) ** (-0.5)
+    for group in range(groups):
+        base = group * batches
+        rows = jnp.concatenate([query[base + b : base + b + 1] for b, _ in place_of], axis=0)
+        wide = [
+            jnp.where((tile_lane + low) // HEAD_LANES == tile_row, rows, 0.0)
+            for low in range(0, depth, LANES)
+        ]
+        fade = jnp.concatenate([forgets[h][base + b : base + b + 1] for b, h in place_of], axis=0)
+        wide = jnp.concatenate(wide, axis=1).astype(BF16)
+        scores = dot(wide, keys[group]) * scale + fade
+        scores = scores + decay[base : base + batches].reshape(per_group, -1)
+        top = jnp.max(scores, axis=1, keepdims=True)
+        short = jnp.exp(scores - top).astype(BF16).astype(F32)
+        total = jnp.sum(short, axis=1, keepdims=True)
+        for row, (b, h) in enumerate(place_of):
+            mixed = jnp.zeros((HEAD_LANES, LANES), F32)
+            for place in range(0, short.shape[1], LANES):
+                value = values[
+                    group, row * HEAD_LANES : (row + 1) * HEAD_LANES, place : place + LANES
+                ]
+                mixed = mixed + value.astype(F32) * short[row : row + 1, place : place + LANES]
+            summed = jnp.sum(mixed, axis=1, keepdims=True)
+            columns = jnp.where(column == h * batch + base + b, summed, columns)
+        stats = jnp.where(tile_lane == group, top, stats)
+        stats = jnp.where(tile_lane == HEAD_LANES + group, total, stats)
+    flat = jnp.concatenate([columns, columns], axis=0).T
+    lane = iota((batch, LANES), 1)
+    part[:batch, :] = jnp.where(lane < HEAD_LANES, flat[:batch], flat[batch : 2 * batch])
+    part[batch:, :] = stats
+
+
+def newest_kernel(normed, queries, key_weight, value_weight, newest, own):
+    rounded = normed[...]
+    key_new = dot(rounded, key_weight[...]).astype(BF16)
+    newest[...] = dot(rounded, value_weight[...]).astype(BF16).astype(F32)
+    product = queries[...].astype(F32) * key_new.astype(F32)
+    low = iota(product.shape, 1) < HEAD_LANES
+    scale = float(HEAD_LANES) ** (-0.5)
+    one = jnp.sum(jnp.where(low, product, 0.0), axis=1, keepdims=True)
+    two = jnp.sum(jnp.where(low, 0.0, product), axis=1, keepdims=True)
+    own[...] = jnp.where(low, one, two) * scale
+
+
+def merge_kernel(local_heads, groups, count, *refs):
+    newest, owns, out_weight, short, full = refs[count:]
+    batch = newest.shape[0]
     batches = batch // groups
-    for group in range(groups):
-        low = group * per_group
-        scores = dot(query_wide[low : low + per_group], keys[group]) * scale
-        fade = decay[group * batches : (group + 1) * batches].reshape(per_group, -1)
-        scores = scores + forget_rows[low : low + per_group] + fade
-        top = jnp.max(scores, axis=1, keepdims=True)
-        weights = jnp.exp(scores - top).astype(BF16)
-        total = jnp.sum(weights.astype(F32), axis=1, keepdims=True)
-        sums = lax.dot_general(
-            weights, values[group], CONTRACT_LAST, preferred_element_type=F32
-        )
-        sums = jnp.where(diagonal, sums, 0.0)
-        folded = sums[:, :LANES]
-        for low_lane in range(LANES, depth, LANES):
-            folded = folded + sums[:, low_lane : low_lane + LANES]
-        folded = folded + pltpu.roll(folded, HEAD_LANES, 1)
-        part[low : low + per_group, :] = jnp.where(
-            lane < HEAD_LANES, folded, jnp.where(lane < 96, top, total)
-        )
-    key_new = dot(rounded, key_weight[...]).astype(BF16)
-    value_new = dot(rounded, value_weight[...]).astype(BF16)
-    product = query.astype(F32) * key_new.astype(F32)
-    mine = iota((rows, LANES), 1) // HEAD_LANES == iota((rows, LANES), 0) % local_heads
-    own = jnp.sum(jnp.where(mine, exact_dot(spread, product), 0.0), axis=1, keepdims=True) * scale
-    value_rows = jnp.where(mine, dot(spread_short, value_new), 0.0)
-    value_rows = value_rows + pltpu.roll(value_rows, HEAD_LANES, 1)
-    newest[...] = jnp.where(iota((rows, LANES), 1) < HEAD_LANES, value_rows, own)
-
-
-def merge_kernel(local_heads, count, *refs):
-    parts = [ref[...] for ref in refs[:count]]
-    newest, out_weight, short, full = refs[count:]
-    rows = newest.shape[0]
-    lane = iota((rows, LANES), 1)
-
-    def pick(array, index):
-        return jnp.sum(jnp.where(lane == index, array, 0.0), axis=1, keepdims=True)
-
-    tops = [pick(array, HEAD_LANES) for array in parts]
-    totals = [pick(array, 96) for array in parts]
-    latest = newest[...]
-    own = pick(latest, HEAD_LANES)
+    lane = iota((batch, LANES), 1)
+    row = iota((batch, LANES), 0)
+    low = lane < HEAD_LANES
+
+    def spread(stats, offset):
+        found = []
+        for head in range(local_heads):
+            picked = stats[head : head + 1]
+            for b in range(1, batches):
+                index = b * local_heads + head
+                picked = jnp.where(row % batches == b, stats[index : index + 1], picked)
+            picked = jnp.where(lane == offset + row // batches, picked, 0.0)
+            found.append(jnp.sum(picked, axis=1, keepdims=True))
+        return jnp.where(low, found[0], found[1])
+
+    tops = [spread(ref[batch:, :], 0) for ref in refs[:count]]
+    totals = [spread(ref[batch:, :], HEAD_LANES) for ref in refs[:count]]
+    own = owns[...]
     peak = own
     for top in tops:
         peak = jnp.maximum(peak, top)
     own_factor = jnp.exp(own - peak)
-    numer = latest * own_factor
+    numer = newest[...] * own_factor
     denom = own_factor
-    for array, top, total in zip(parts, tops, totals):
+    for ref, top, total in zip(refs, tops, totals):
         factor = jnp.exp(top - peak)
-        numer = numer + array * factor
+        numer = numer + ref[:batch, :] * factor
         denom = denom + total * factor
-    ratio = jnp.where(lane < HEAD_LANES, numer / denom, 0.0)
-    ratio = ratio + pltpu.roll(ratio, HEAD_LANES, 1)
-    mine = lane // HEAD_LANES == iota((rows, LANES), 0) % local_heads
-    ratio = jnp.where(mine, ratio, 0.0).astype(BF16)
-    batch = rows // local_heads
-    gather = (iota((batch, rows), 1) // local_heads == iota((batch, rows), 0)).astype(BF16)
-    attention = dot(gather, ratio).astype(BF16)
-    product = dot(attention, out_weight[...])
+    product = dot((numer / denom).astype(BF16), out_weight[...])
     full[...] = product
     short[...] = product.astype(BF16)
 
@@ -316,30 +324,44 @@
     product = dot(mixed[...], up_weight[...])
     width = product.shape[1]
     full[...] = product
-    short[:, :width] = product.astype(BF16)
+    for block in range(width // LANES):
+        short[block * batch : (block + 1) * batch, :] = product[
+            :, block * LANES : (block + 1) * LANES
+        ].astype(BF16)
     rest = jnp.sum(squares, axis=1, keepdims=True)
     lane = iota((batch, LANES), 1)
-    tail = jnp.zeros((batch, LANES), F32)
+    rest = jnp.where(lane == iota((batch, LANES), 0), rest, 0.0)
+    rest = jnp.sum(rest, axis=0, keepdims=True)
+    row = iota((PACK, LANES), 0)
+    tail = jnp.zeros((PACK, LANES), F32)
     for index in range(3):
         digit = rest.astype(BF16).astype(F32)
-        tail = jnp.where(lane == index, digit, tail)
+        tail = jnp.where(row == index, digit, tail)
         rest = rest - digit
-    short[:, width:] = tail.astype(BF16)
+    short[short.shape[0] - PACK :, :] = tail.astype(BF16)
 
 
 def down_kernel(tp, size, count, *refs):
     full, short = refs[0], refs[1]
     others = refs[2 : 1 + count]
     down_weight, keep, send, shares = refs[1 + count :]
-    width = full.shape[1]
-    total = full[...]
-    tail = short[:, width:].astype(F32)
+    batch, width = full.shape
+    height = width // LANES * batch
+    tail = short[height:, :].astype(F32)
     for ref in others:
-        total = total + ref[:, :width].astype(F32)
-        tail = tail + ref[:, width:].astype(F32)
-    mean = jnp.sum(tail, axis=1, keepdims=True) / size
-    active = jnp.maximum(total * lax.rsqrt(mean + EPS), 0.0)
-    product = dot((active * active).astype(BF16), down_weight[...])
+        tail = tail + ref[height:, :].astype(F32)
+    tail = jnp.sum(tail, axis=0, keepdims=True)
+    lane = iota((batch, LANES), 1)
+    tail = jnp.where(lane == iota((batch, LANES), 0), tail, 0.0)
+    inverse = lax.rsqrt(jnp.sum(tail, axis=1, keepdims=True) / size + EPS)
+    pieces = []
+    for block in range(width // LANES):
+        total = full[:, block * LANES : (block + 1) * LANES]
+        for ref in others:
+            total = total + ref[block * batch : (block + 1) * batch, :].astype(F32)
+        active = jnp.maximum(total * inverse, 0.0)
+        pieces.append((active * active).astype(BF16))
+    product = dot(jnp.concatenate(pieces, axis=1), down_weight[...])
     for block in range(tp):
         shares[block] = product[:, block * LANES : (block + 1) * LANES]
     core = lax.rem(lax.axis_index("tp"), 2)
@@ -390,7 +412,10 @@
         and head_size == HEAD_LANES
         and local_heads == LANES // HEAD_LANES
         and tp % 2 == 0
-        and rows % 8 == 0
+        and kv & (kv - 1) == 0
+        and rows == HEAD_LANES
+        and batch % PACK == 0
+        and up_weight.shape[1] % LANES == 0
         and places % LANES == 0
         and out_weight.shape[1] == tp * LANES
     )
@@ -425,52 +450,60 @@
     keys = jnp.swapaxes(key_cache, 2, 3).reshape(groups, depth, places)
     values = jnp.swapaxes(value_cache, 2, 3).reshape(groups, depth, places)
     heads = forget_bias.shape[0]
-    part, newest = kernel_call(
+    part, normed, queries = kernel_call(
         functools.partial(attention_kernel, local_heads),
-        [shape_of((rows, LANES), F32)] * 2,
+        [
+            shape_of((batch + 8, LANES), F32),
+            shape_of((batch, size), BF16),
+            shape_of((batch, LANES), BF16),
+        ],
         (
             blocks,
             mixer_gain.reshape(count, LANES),
             query_weight,
-            key_weight,
-            value_weight,
             forget_weight.T,
             forget_bias.reshape(1, heads),
             keys,
             values,
             past_decay,
         ),
-        scratch=[pltpu.VMEM((batch, size), BF16)],
-    )
-    def turn(array, axis, length, step, stride=1):
-        total = length * stride
-        return lax.ppermute(array, axis, [(i, (i + step * stride) % total) for i in range(total)])
+    )
+    newest, owns = kernel_call(
+        newest_kernel,
+        [shape_of((batch, LANES), F32)] * 2,
+        (normed, queries, key_weight, value_weight),
+    )
+    def trade(array, step):
+        return lax.ppermute(array, "kv", [(i, i ^ step) for i in range(kv)])
+
+    def turn(array, step):
+        return lax.ppermute(array, "tp", [(i, (i + 2 * step) % tp) for i in range(tp)])
 
     def swap(array):
         return lax.ppermute(array, "tp", [(i, i ^ 1) for i in range(tp)])
 
     pairs = tp // 2
-    others = [turn(part, "kv", kv, step) for step in range(1, kv)]
+    others = [trade(part, step) for step in range(1, kv)]
     block_width = out_weight.shape[1]
     short, full = kernel_call(
-        functools.partial(merge_kernel, local_heads, kv),
+        functools.partial(merge_kernel, local_heads, groups, kv),
         [shape_of((batch, block_width), BF16), shape_of((batch, block_width), F32)],
-        (part, *others, newest, out_weight),
-    )
-    others = [turn(short, "tp", pairs, step, 2) for step in range(1, pairs)]
+        (part, *others, newest, owns, out_weight),
+    )
+    others = [turn(short, step) for step in range(1, pairs)]
     (column_sum,) = kernel_call(add_kernel, [shape_of((batch, block_width), F32)], (full, *others))
     width = up_weight.shape[1]
     short, full, piece = kernel_call(
         functools.partial(up_kernel, kv, tp),
         [
-            shape_of((batch, width + LANES), BF16),
+            shape_of((batch * width // LANES + PACK, LANES), BF16),
             shape_of((batch, width), F32),
             shape_of((batch, LANES), F32),
         ],
         (column_sum, swap(column_sum), blocks, channel_gain.reshape(count, LANES), up_weight),
         scratch=[pltpu.VMEM((tp, batch, LANES), F32), pltpu.VMEM((batch, block_width), BF16)],
     )
-    others = [turn(short, "kv", kv, step) for step in range(1, kv)]
+    others = [trade(short, step) for step in range(1, kv)]
     keep, send = kernel_call(
         functools.partial(down_kernel, tp, size, kv),
         [shape_of((pairs, batch, LANES), F32)] * 2,
@@ -483,7 +516,7 @@
         (keep, swap(send)),
         scratch=[pltpu.VMEM((pairs, batch, LANES), F32)],
     )
-    others = [turn(shares[step - 1], "tp", pairs, step, 2) for step in range(1, pairs)]
+    others = [turn(shares[step - 1], step) for step in range(1, pairs)]
     (updated,) = kernel_call(
         last_kernel, [shape_of((batch, LANES), BF16)], (piece, own, *others)
     )

time: 60.5 us -> 56.8 us (0.939)
  waiting for transfers between devices: 20.1 us -> 17.3 us
  Pallas kernels: 8.68 us -> 6.44 us
  starting transfers between devices: 13.3 us -> 14.6 us
    ppermute x12, waiting for transfers between devices: 17.6 us -> 14.7 us  [the longest x6 8.14 us: trade(): return lax.ppermute(array, 'kv', [(i, i ^ step) for i in range(kv)])]
    pallas_call x8 -> x9, Pallas kernels: 8.68 us -> 6.44 us  [kernel_call(): pl.pallas_call(body, out_shape=tuple(out_shapes), in_specs=[pl.BlockSpec(...]
    ppermute x12, starting transfers between devices: 13.1 us -> 14.5 us  [the longest x6 7.41 us: turn(): lax.ppermute(array, 'tp', [(i, (i + 2 * step) % tp) for i in range(tp)])]
  transfers between devices with their start and end apart: 14 -> 14, of which waited for: 11 -> 11; matrix products, arithmetic and copies ran while one was open for 0% -> 0% of each run, Pallas kernels for 0% -> 1%
where the time goes in v2:
time: 56.8 us; the launch traced here: 56.6 us
  waiting for transfers between devices  17.3 us (30%)
  blocking collectives  17.1 us (30%)
  starting transfers between devices  14.6 us (26%)
  Pallas kernels  6.44 us (11%)
  local copies, waits for them, and re-layouts  0.92 us (2%)
    all_to_all x1, blocking collectives, shards(): blocks = lax.all_to_all(fanned, ('kv', 'tp'), 0, 0)  17.1 us
    ppermute x6, waiting for transfers between devices, trade(): return lax.ppermute(array, 'kv', [(i, i ^ step) for i in range(kv)])  8.14 us
    ppermute x6, starting transfers between devices, turn(): lax.ppermute(array, 'tp', [(i, (i + 2 * step) % tp) for i in range(tp)])  7.41 us
    ppermute x6, starting transfers between devices, trade(): return lax.ppermute(array, 'kv', [(i, i ^ step) for i in range(kv)])  7.07 us
    ppermute x6, waiting for transfers between devices, turn(): lax.ppermute(array, 'tp', [(i, (i + 2 * step) % tp) for i in range(tp)])  6.59 us
    pallas_call x9, Pallas kernels, kernel_call(): pl.pallas_call(body, out_shape=tuple(out_shapes), in_specs=[pl.BlockSpec(...  6.44 us
    ppermute x2, waiting for transfers between devices, swap(): return lax.ppermute(array, 'tp', [(i, i ^ 1) for i in range(tp)])  2.57 us
  transfers between devices with their start and end apart: 14, of which 11 were waited for; matrix products, arithmetic and copies ran while one was open for 0% of the time, Pallas kernels for 1%

profile of v2, /device:TPU:0, one launch (start us, length us, event | category | flops | bytes accessed | tf_op | source)
XLA Modules:
  0.0 56.6 jit_solution(16971530875584918473)
XLA Ops:
  0.0 0.8 %copy-done.13 = bf16[32,128]{1,0:T(8,128)(2,1)S(1)} copy-done((bf16[32,128]{1,0:T(8,128)(2,1)S(1)}, bf16[32,128]{1,0:T(8,128)(2,1)}, u32[]{:S(2)}) %copy-start.13) | copy-done | bytes 8216
  0.9 17.1 %all_to_all.5.blocks = bf16[32,32,128]{2,1,0:T(8,128)(2,1)S(1)} all-to-all(bf16[32,32,128]{2,1,0:T(8,128)(2,1)S(1)} %shard_map.136), channel_id=1, replica_groups=mesh['kv'=4,'tp'=8] {'kv','tp'}, dimensions={0} | all-to-all | bytes 524288 | tf_op jit(solution)/shard_map/all_to_all | solution.py:449
  18.2 3.3 %shard_map.137 = (f32[40,128]{1,0:T(8,128)S(1)}, bf16[32,4096]{1,0:T(8,128)(2,1)S(1)}, bf16[32,128]{1,0:T(8,128)(2,1)S(1)}) custom-call(bf16[32,32,128]{2,1,0:T(8,128)(2,1)S(1)} %all_to_all.5.blocks, f32[32,128]{1,0:T(8,128)S(1)} %bitcast.13, bf16[4096,128]{1,0:T(8,128)(2,1)S(1)} %copy-done.4, bf16[16,4096]{1,0:T(8,128)(2,1)S(1)} %bitcast.12, ...), custom_call_target="tpu_custom_call" | custom-call | tf_op jit(solution)/shard_map/pallas_call | solution.py:154
  21.5 1.2 %collective-permute-start.2 = (f32[40,128]{1,0:T(8,128)S(1)}, f32[40,128]{1,0:T(8,128)S(1)}, u32[]{:S(2)}, u32[]{:S(2)}) collective-permute-start(f32[40,128]{1,0:T(8,128)S(1)} %get-tuple-element.21.refs_0_), channel_id=1, source_target_pairs={{0,24},{8,16},{16,8},{24,0},{1,25},{9,17},{17,9},{25,1},{2,26},{10... | collective-permute-start | bytes 61448 | tf_op jit(solution)/shard_map/ppermute | solution.py:477
  22.7 1.2 %collective-permute-start.1 = (f32[40,128]{1,0:T(8,128)S(1)}, f32[40,128]{1,0:T(8,128)S(1)}, u32[]{:S(2)}, u32[]{:S(2)}) collective-permute-start(f32[40,128]{1,0:T(8,128)S(1)} %get-tuple-element.21.refs_0_), channel_id=1, source_target_pairs={{0,16},{8,24},{16,0},{24,8},{1,17},{9,25},{17,1},{25,9},{2,18},{10... | collective-permute-start | bytes 61448 | tf_op jit(solution)/shard_map/ppermute | solution.py:477
  23.9 1.2 %collective-permute-start = (f32[40,128]{1,0:T(8,128)S(1)}, f32[40,128]{1,0:T(8,128)S(1)}, u32[]{:S(2)}, u32[]{:S(2)}) collective-permute-start(f32[40,128]{1,0:T(8,128)S(1)} %get-tuple-element.21.refs_0_), channel_id=1, source_target_pairs={{0,8},{8,0},{16,24},{24,16},{1,9},{9,1},{17,25},{25,17},{2,10},{10... | collective-permute-start | bytes 61448 | tf_op jit(solution)/shard_map/ppermute | solution.py:477
  25.5 0.8 %collective-permute-done.2.refs_3_ = f32[40,128]{1,0:T(8,128)S(1)} collective-permute-done((f32[40,128]{1,0:T(8,128)S(1)}, f32[40,128]{1,0:T(8,128)S(1)}, u32[]{:S(2)}, u32[]{:S(2)}) %collective-permute-start.2) | collective-permute-done | bytes 20512 | tf_op jit(solution)/shard_map/ppermute | solution.py:477
  26.5 1.2 %collective-permute-done.refs_1_ = f32[40,128]{1,0:T(8,128)S(1)} collective-permute-done((f32[40,128]{1,0:T(8,128)S(1)}, f32[40,128]{1,0:T(8,128)S(1)}, u32[]{:S(2)}, u32[]{:S(2)}) %collective-permute-start) | collective-permute-done | bytes 20512 | tf_op jit(solution)/shard_map/ppermute | solution.py:477
  28.0 1.4 %collective-permute-start.5 = (bf16[32,1024]{1,0:T(8,128)(2,1)S(1)}, bf16[32,1024]{1,0:T(8,128)(2,1)S(1)}, u32[]{:S(2)}, u32[]{:S(2)}) collective-permute-start(bf16[32,1024]{1,0:T(8,128)(2,1)S(1)} %get-tuple-element.27), channel_id=1, source_target_pairs={{0,6},{1,7},{2,0},{3,1},{4,2},{5,3},{6,4},{7,5},{8,14},{9,15},{10,... | collective-permute-start | bytes 196616 | tf_op jit(solution)/shard_map/ppermute | solution.py:480
  29.4 1.8 %collective-permute-start.3 = (bf16[32,1024]{1,0:T(8,128)(2,1)S(1)}, bf16[32,1024]{1,0:T(8,128)(2,1)S(1)}, u32[]{:S(2)}, u32[]{:S(2)}) collective-permute-start(bf16[32,1024]{1,0:T(8,128)(2,1)S(1)} %get-tuple-element.27), channel_id=1, source_target_pairs={{0,2},{1,3},{2,4},{3,5},{4,6},{5,7},{6,0},{7,1},{8,10},{9,11},{10,... | collective-permute-start | bytes 196616 | tf_op jit(solution)/shard_map/ppermute | solution.py:480
  31.2 1.4 %collective-permute-done.5.refs_3_ = bf16[32,1024]{1,0:T(8,128)(2,1)S(1)} collective-permute-done((bf16[32,1024]{1,0:T(8,128)(2,1)S(1)}, bf16[32,1024]{1,0:T(8,128)(2,1)S(1)}, u32[]{:S(2)}, u32[]{:S(2)}) %collective-permute-start.5) | collective-permute-done | bytes 65568 | tf_op jit(solution)/shard_map/ppermute | solution.py:480
  32.6 3.4 %collective-permute-done.4.refs_2_ = bf16[32,1024]{1,0:T(8,128)(2,1)S(1)} collective-permute-done((bf16[32,1024]{1,0:T(8,128)(2,1)S(1)}, bf16[32,1024]{1,0:T(8,128)(2,1)S(1)}, u32[]{:S(2)}, u32[]{:S(2)}) %collective-permute-start.4) | collective-permute-done | bytes 65568 | tf_op jit(solution)/shard_map/ppermute | solution.py:480
  36.0 1.3 %collective-permute-done.6.two = f32[32,1024]{1,0:T(8,128)S(1)} collective-permute-done((f32[32,1024]{1,0:T(8,128)S(1)}, f32[32,1024]{1,0:T(8,128)S(1)}, u32[]{:S(2)}, u32[]{:S(2)}) %collective-permute-start.6) | collective-permute-done | bytes 131104 | tf_op jit(solution)/shard_map/ppermute | solution.py:483
  37.4 0.8 %shard_map.141 = (bf16[528,128]{1,0:T(8,128)(2,1)S(1)}, f32[32,2048]{1,0:T(8,128)S(1)}, f32[32,128]{1,0:T(8,128)S(1)}) custom-call(f32[32,1024]{1,0:T(8,128)S(1)} %shard_map.140.one, f32[32,1024]{1,0:T(8,128)S(1)} %collective-permute-done.6.two, bf16[32,32,128]{2,1,0:T(8,128)(2,1)S(1)} %all_to_all.5.blocks, f32[32,128]{1,0:T(8,128)S(1)} %bitcast.14, ...), custom_call_target="tpu_custom_call" | custom-call | tf_op jit(solution)/shard_map/pallas_call | solution.py:154
  38.2 1.9 %collective-permute-start.9 = (bf16[528,128]{1,0:T(8,128)(2,1)S(1)}, bf16[528,128]{1,0:T(8,128)(2,1)S(1)}, u32[]{:S(2)}, u32[]{:S(2)}) collective-permute-start(bf16[528,128]{1,0:T(8,128)(2,1)S(1)} %get-tuple-element.30.refs_1_), channel_id=1, source_target_pairs={{0,24},{8,16},{16,8},{24,0},{1,25},{9,17},{17,9},{25,1},{2,26},{10... | collective-permute-start | bytes 405512 | tf_op jit(solution)/shard_map/ppermute | solution.py:477
  40.1 1.2 %collective-permute-start.8 = (bf16[528,128]{1,0:T(8,128)(2,1)S(1)}, bf16[528,128]{1,0:T(8,128)(2,1)S(1)}, u32[]{:S(2)}, u32[]{:S(2)}) collective-permute-start(bf16[528,128]{1,0:T(8,128)(2,1)S(1)} %get-tuple-element.30.refs_1_), channel_id=1, source_target_pairs={{0,16},{8,24},{16,0},{24,8},{1,17},{9,25},{17,1},{25,9},{2,18},{10... | collective-permute-start | bytes 405512 | tf_op jit(solution)/shard_map/ppermute | solution.py:477
  41.7 3.9 %collective-permute-done.9.refs_4_ = bf16[528,128]{1,0:T(8,128)(2,1)S(1)} collective-permute-done((bf16[528,128]{1,0:T(8,128)(2,1)S(1)}, bf16[528,128]{1,0:T(8,128)(2,1)S(1)}, u32[]{:S(2)}, u32[]{:S(2)}) %collective-permute-start.9) | collective-permute-done | bytes 135200 | tf_op jit(solution)/shard_map/ppermute | solution.py:477
  45.6 2.1 %collective-permute-done.8.refs_3_ = bf16[528,128]{1,0:T(8,128)(2,1)S(1)} collective-permute-done((bf16[528,128]{1,0:T(8,128)(2,1)S(1)}, bf16[528,128]{1,0:T(8,128)(2,1)S(1)}, u32[]{:S(2)}, u32[]{:S(2)}) %collective-permute-start.8) | collective-permute-done | bytes 135200 | tf_op jit(solution)/shard_map/ppermute | solution.py:477
  47.7 0.9 %shard_map.142 = (f32[4,32,128]{2,1,0:T(8,128)S(1)}, f32[4,32,128]{2,1,0:T(8,128)S(1)}) custom-call(f32[32,2048]{1,0:T(8,128)S(1)} %get-tuple-element.29.refs_0_, bf16[528,128]{1,0:T(8,128)(2,1)S(1)} %get-tuple-element.30.refs_1_, bf16[528,128]{1,0:T(8,128)(2,1)S(1)} %collective-permute-done.7.refs_2_, bf16[528,128]{1,0:T(8,128)(2,1)S(1)} %collective-permute-done.8.refs_3_, ...), custom_call_target="tpu_custom_call" | custom-call | tf_op jit(solution)/shard_map/pallas_call | solution.py:154
  48.7 1.2 %collective-permute-done.10.other = f32[4,32,128]{2,1,0:T(8,128)S(1)} collective-permute-done((f32[4,32,128]{2,1,0:T(8,128)S(1)}, f32[4,32,128]{2,1,0:T(8,128)S(1)}, u32[]{:S(2)}, u32[]{:S(2)}) %collective-permute-start.10) | collective-permute-done | bytes 65568 | tf_op jit(solution)/shard_map/ppermute | solution.py:483
  50.0 2.0 %collective-permute-start.12 = (bf16[32,128]{1,0:T(8,128)(2,1)S(1)}, bf16[32,128]{1,0:T(8,128)(2,1)S(1)}, u32[]{:S(2)}, u32[]{:S(2)}) collective-permute-start(bf16[32,128]{1,0:T(8,128)(2,1)S(1)} %get-tuple-element.35), channel_id=1, source_target_pairs={{0,4},{1,5},{2,6},{3,7},{4,0},{5,1},{6,2},{7,3},{8,12},{9,13},{10,... | collective-permute-start | bytes 24584 | tf_op jit(solution)/shard_map/ppermute | solution.py:480
  52.0 2.1 %collective-permute-start.13 = (bf16[32,128]{1,0:T(8,128)(2,1)S(1)}, bf16[32,128]{1,0:T(8,128)(2,1)S(1)}, u32[]{:S(2)}, u32[]{:S(2)}) collective-permute-start(bf16[32,128]{1,0:T(8,128)(2,1)S(1)} %get-tuple-element.36), channel_id=1, source_target_pairs={{0,6},{1,7},{2,0},{3,1},{4,2},{5,3},{6,4},{7,5},{8,14},{9,15},{10,... | collective-permute-start | bytes 24584 | tf_op jit(solution)/shard_map/ppermute | solution.py:480
  54.1 1.3 %collective-permute-done.11.refs_2_ = bf16[32,128]{1,0:T(8,128)(2,1)S(1)} collective-permute-done((bf16[32,128]{1,0:T(8,128)(2,1)S(1)}, bf16[32,128]{1,0:T(8,128)(2,1)S(1)}, u32[]{:S(2)}, u32[]{:S(2)}) %collective-permute-start.11) | collective-permute-done | bytes 8224 | tf_op jit(solution)/shard_map/ppermute | solution.py:480
  56.0 0.6 %shard_map.144 = bf16[32,128]{1,0:T(8,128)(2,1)} custom-call(f32[32,128]{1,0:T(8,128)S(1)} %get-tuple-element.28.refs_0_, f32[32,128]{1,0:T(8,128)S(1)} %get-tuple-element.33.refs_1_, bf16[32,128]{1,0:T(8,128)(2,1)S(1)} %collective-permute-done.11.refs_2_, bf16[32,128]{1,0:T(8,128)(2,1)S(1)} %collective-permute-done.12.refs_3_, ...), custom_call_target="tpu_custom_call" | custom-call | tf_op jit(solution)/shard_map/pallas_call | solution.py:154
  (42 shorter events, 2.3 us)
Async XLA Ops:
  0.0 18.1 %copy-start.7 = (f32[32,2,1024]{2,1,0:T(2,128)S(1)}, f32[32,2,1024]{2,1,0:T(2,128)}, u32[]{:S(2)}) copy-start(f32[32,2,1024]{2,1,0:T(2,128)} %decay.1) | copy-start | bytes 786436
  0.0 18.1 %copy-start.1 = (bf16[32,2,1024,64]{2,3,1,0:T(8,128)(2,1)S(1)}, bf16[32,2,1024,64]{2,3,1,0:T(8,128)(2,1)}, u32[]{:S(2)}) copy-start(bf16[32,2,1024,64]{2,3,1,0:T(8,128)(2,1)} %param.22) | copy-start | bytes 25165828
  0.0 18.1 %copy-start = (bf16[32,2,1024,64]{2,3,1,0:T(8,128)(2,1)S(1)}, bf16[32,2,1024,64]{2,3,1,0:T(8,128)(2,1)}, u32[]{:S(2)}) copy-start(bf16[32,2,1024,64]{2,3,1,0:T(8,128)(2,1)} %param.21) | copy-start | bytes 25165828
  0.0 18.1 %copy-start.12 = (f32[16]{0:T(128)S(1)}, f32[16]{0:T(128)}, u32[]{:S(2)}) copy-start(f32[16]{0:T(128)} %param.20) | copy-start | bytes 196
  0.0 18.1 %copy-start.9 = (bf16[4096,16]{0,1:T(8,128)(2,1)S(1)}, bf16[4096,16]{0,1:T(8,128)(2,1)}, u32[]{:S(2)}) copy-start(bf16[4096,16]{0,1:T(8,128)(2,1)} %param.19) | copy-start | bytes 393220
  0.0 18.1 %copy-start.4 = (bf16[4096,128]{1,0:T(8,128)(2,1)S(1)}, bf16[4096,128]{1,0:T(8,128)(2,1)}, u32[]{:S(2)}) copy-start(bf16[4096,128]{1,0:T(8,128)(2,1)} %query_weight.1) | copy-start | bytes 3145732
  0.0 18.1 %copy-start.10 = (f32[4096]{0:T(1024)S(1)}, f32[4096]{0:T(1024)}, u32[]{:S(2)}) copy-start(f32[4096]{0:T(1024)} %param.15) | copy-start | bytes 49156
  18.2 19.2 %copy-start.2 = (bf16[1024,2048]{1,0:T(8,128)(2,1)S(1)}, bf16[1024,2048]{1,0:T(8,128)(2,1)}, u32[]{:S(2)}) copy-start(bf16[1024,2048]{1,0:T(8,128)(2,1)} %up_weight.1) | copy-start | bytes 12582916
  18.2 19.2 %copy-start.11 = (f32[4096]{0:T(1024)S(1)}, f32[4096]{0:T(1024)}, u32[]{:S(2)}) copy-start(f32[4096]{0:T(1024)} %param.25) | copy-start | bytes 49156
  21.5 26.2 %copy-start.3 = (bf16[2048,1024]{1,0:T(8,128)(2,1)S(1)}, bf16[2048,1024]{1,0:T(8,128)(2,1)}, u32[]{:S(2)}) copy-start(bf16[2048,1024]{1,0:T(8,128)(2,1)} %refs_5_.1) | copy-start | bytes 12582916
  21.5 4.7 %collective-permute-start.2 = (f32[40,128]{1,0:T(8,128)S(1)}, f32[40,128]{1,0:T(8,128)S(1)}, u32[]{:S(2)}, u32[]{:S(2)}) collective-permute-start(f32[40,128]{1,0:T(8,128)S(1)} %get-tuple-element.21.refs_0_), channel_id=1, source_target_pairs={{0,24},{8,16},{16,8},{24,0},{1,25},{9,17},{17,9},{25,1},{2,26},{10... | collective-permute-start | bytes 61448 | tf_op jit(solution)/shard_map/ppermute | solution.py:477
  22.7 3.8 %collective-permute-start.1 = (f32[40,128]{1,0:T(8,128)S(1)}, f32[40,128]{1,0:T(8,128)S(1)}, u32[]{:S(2)}, u32[]{:S(2)}) collective-permute-start(f32[40,128]{1,0:T(8,128)S(1)} %get-tuple-element.21.refs_0_), channel_id=1, source_target_pairs={{0,16},{8,24},{16,0},{24,8},{1,17},{9,25},{17,1},{25,9},{2,18},{10... | collective-permute-start | bytes 61448 | tf_op jit(solution)/shard_map/ppermute | solution.py:477
  23.9 3.8 %collective-permute-start = (f32[40,128]{1,0:T(8,128)S(1)}, f32[40,128]{1,0:T(8,128)S(1)}, u32[]{:S(2)}, u32[]{:S(2)}) collective-permute-start(f32[40,128]{1,0:T(8,128)S(1)} %get-tuple-element.21.refs_0_), channel_id=1, source_target_pairs={{0,8},{8,0},{16,24},{24,16},{1,9},{9,1},{17,25},{25,17},{2,10},{10... | collective-permute-start | bytes 61448 | tf_op jit(solution)/shard_map/ppermute | solution.py:477
  28.0 4.6 %collective-permute-start.5 = (bf16[32,1024]{1,0:T(8,128)(2,1)S(1)}, bf16[32,1024]{1,0:T(8,128)(2,1)S(1)}, u32[]{:S(2)}, u32[]{:S(2)}) collective-permute-start(bf16[32,1024]{1,0:T(8,128)(2,1)S(1)} %get-tuple-element.27), channel_id=1, source_target_pairs={{0,6},{1,7},{2,0},{3,1},{4,2},{5,3},{6,4},{7,5},{8,14},{9,15},{10,... | collective-permute-start | bytes 196616 | tf_op jit(solution)/shard_map/ppermute | solution.py:480
  29.3 6.6 %collective-permute-start.4 = (bf16[32,1024]{1,0:T(8,128)(2,1)S(1)}, bf16[32,1024]{1,0:T(8,128)(2,1)S(1)}, u32[]{:S(2)}, u32[]{:S(2)}) collective-permute-start(bf16[32,1024]{1,0:T(8,128)(2,1)S(1)} %get-tuple-element.27), channel_id=1, source_target_pairs={{0,4},{1,5},{2,6},{3,7},{4,0},{5,1},{6,2},{7,3},{8,12},{9,13},{10,... | collective-permute-start | bytes 196616 | tf_op jit(solution)/shard_map/ppermute | solution.py:480
  29.4 6.5 %collective-permute-start.3 = (bf16[32,1024]{1,0:T(8,128)(2,1)S(1)}, bf16[32,1024]{1,0:T(8,128)(2,1)S(1)}, u32[]{:S(2)}, u32[]{:S(2)}) collective-permute-start(bf16[32,1024]{1,0:T(8,128)(2,1)S(1)} %get-tuple-element.27), channel_id=1, source_target_pairs={{0,2},{1,3},{2,4},{3,5},{4,6},{5,7},{6,0},{7,1},{8,10},{9,11},{10,... | collective-permute-start | bytes 196616 | tf_op jit(solution)/shard_map/ppermute | solution.py:480
  36.0 1.4 %collective-permute-start.6 = (f32[32,1024]{1,0:T(8,128)S(1)}, f32[32,1024]{1,0:T(8,128)S(1)}, u32[]{:S(2)}, u32[]{:S(2)}) collective-permute-start(f32[32,1024]{1,0:T(8,128)S(1)} %shard_map.140.one), channel_id=1, source_target_pairs={{0,1},{1,0},{2,3},{3,2},{4,5},{5,4},{6,7},{7,6},{8,9},{9,8},{10,11... | collective-permute-start | bytes 393224 | tf_op jit(solution)/shard_map/ppermute | solution.py:483
  38.2 7.4 %collective-permute-start.9 = (bf16[528,128]{1,0:T(8,128)(2,1)S(1)}, bf16[528,128]{1,0:T(8,128)(2,1)S(1)}, u32[]{:S(2)}, u32[]{:S(2)}) collective-permute-start(bf16[528,128]{1,0:T(8,128)(2,1)S(1)} %get-tuple-element.30.refs_1_), channel_id=1, source_target_pairs={{0,24},{8,16},{16,8},{24,0},{1,25},{9,17},{17,9},{25,1},{2,26},{10... | collective-permute-start | bytes 405512 | tf_op jit(solution)/shard_map/ppermute | solution.py:477
  40.1 7.5 %collective-permute-start.8 = (bf16[528,128]{1,0:T(8,128)(2,1)S(1)}, bf16[528,128]{1,0:T(8,128)(2,1)S(1)}, u32[]{:S(2)}, u32[]{:S(2)}) collective-permute-start(bf16[528,128]{1,0:T(8,128)(2,1)S(1)} %get-tuple-element.30.refs_1_), channel_id=1, source_target_pairs={{0,16},{8,24},{16,0},{24,8},{1,17},{9,25},{17,1},{25,9},{2,18},{10... | collective-permute-start | bytes 405512 | tf_op jit(solution)/shard_map/ppermute | solution.py:477
  41.4 6.3 %collective-permute-start.7 = (bf16[528,128]{1,0:T(8,128)(2,1)S(1)}, bf16[528,128]{1,0:T(8,128)(2,1)S(1)}, u32[]{:S(2)}, u32[]{:S(2)}) collective-permute-start(bf16[528,128]{1,0:T(8,128)(2,1)S(1)} %get-tuple-element.30.refs_1_), channel_id=1, source_target_pairs={{0,8},{8,0},{16,24},{24,16},{1,9},{9,1},{17,25},{25,17},{2,10},{10... | collective-permute-start | bytes 405512 | tf_op jit(solution)/shard_map/ppermute | solution.py:477
  48.6 1.3 %collective-permute-start.10 = (f32[4,32,128]{2,1,0:T(8,128)S(1)}, f32[4,32,128]{2,1,0:T(8,128)S(1)}, u32[]{:S(2)}, u32[]{:S(2)}) collective-permute-start(f32[4,32,128]{2,1,0:T(8,128)S(1)} %get-tuple-element.32), channel_id=1, source_target_pairs={{0,1},{1,0},{2,3},{3,2},{4,5},{5,4},{6,7},{7,6},{8,9},{9,8},{10,11... | collective-permute-start | bytes 196616 | tf_op jit(solution)/shard_map/ppermute | solution.py:483
  49.9 5.5 %collective-permute-start.11 = (bf16[32,128]{1,0:T(8,128)(2,1)S(1)}, bf16[32,128]{1,0:T(8,128)(2,1)S(1)}, u32[]{:S(2)}, u32[]{:S(2)}) collective-permute-start(bf16[32,128]{1,0:T(8,128)(2,1)S(1)} %get-tuple-element.34), channel_id=1, source_target_pairs={{0,2},{1,3},{2,4},{3,5},{4,6},{5,7},{6,0},{7,1},{8,10},{9,11},{10,... | collective-permute-start | bytes 24584 | tf_op jit(solution)/shard_map/ppermute | solution.py:480
  50.0 5.4 %collective-permute-start.12 = (bf16[32,128]{1,0:T(8,128)(2,1)S(1)}, bf16[32,128]{1,0:T(8,128)(2,1)S(1)}, u32[]{:S(2)}, u32[]{:S(2)}) collective-permute-start(bf16[32,128]{1,0:T(8,128)(2,1)S(1)} %get-tuple-element.35), channel_id=1, source_target_pairs={{0,4},{1,5},{2,6},{3,7},{4,0},{5,1},{6,2},{7,3},{8,12},{9,13},{10,... | collective-permute-start | bytes 24584 | tf_op jit(solution)/shard_map/ppermute | solution.py:480
  52.0 4.0 %collective-permute-start.13 = (bf16[32,128]{1,0:T(8,128)(2,1)S(1)}, bf16[32,128]{1,0:T(8,128)(2,1)S(1)}, u32[]{:S(2)}, u32[]{:S(2)}) collective-permute-start(bf16[32,128]{1,0:T(8,128)(2,1)S(1)} %get-tuple-element.36), channel_id=1, source_target_pairs={{0,6},{1,7},{2,0},{3,1},{4,2},{5,3},{6,4},{7,5},{8,14},{9,15},{10,... | collective-permute-start | bytes 24584 | tf_op jit(solution)/shard_map/ppermute | solution.py:480
  (4 other events, 24.3 us)

commit v3 on v2

--- a/solution.py
+++ b/solution.py
@@ -137,6 +137,8 @@
 LANES = 128
 HEAD_LANES = 64
 PACK = 16
+WIDE = 256
+AHEAD = 1
 F32 = jnp.float32
 BF16 = jnp.bfloat16
 CONTRACT_LAST = (((1,), (1,)), ((), ()))
@@ -150,7 +152,7 @@
     return jnp.dot(one, two, preferred_element_type=F32)
 
 
-def kernel_call(body, out_shapes, arguments, scratch=(), limit=8, cost=None):
+def kernel_call(body, out_shapes, arguments, scratch=(), limit=8, cost=None, aliases=None):
     return pl.pallas_call(
         body,
         out_shape=tuple(out_shapes),
@@ -158,6 +160,7 @@
         out_specs=tuple(pl.BlockSpec(memory_space=pltpu.VMEM) for _ in out_shapes),
         scratch_shapes=list(scratch),
         cost_estimate=cost,
+        input_output_aliases=aliases or {},
         compiler_params=pltpu.CompilerParams(vmem_limit_bytes=limit << 20),
     )(*arguments)
 
@@ -170,6 +173,10 @@
     value = piece[...]
     for index in range(copies.shape[0]):
         copies[index] = value
+
+
+def hold_kernel(copies, same):
+    same[0] = copies[0]
 
 
 def attention_kernel(
@@ -185,6 +192,7 @@
     part,
     normed,
     queries,
+    spread,
 ):
     groups, depth, _ = keys.shape
     count, batch, _ = blocks.shape
@@ -221,7 +229,8 @@
     columns = jnp.zeros((HEAD_LANES, LANES), F32)
     stats = jnp.zeros((per_group, LANES), F32)
     scale = float(HEAD_LANES) ** (-0.5)
-    for group in range(groups):
+
+    def weigh(group):
         base = group * batches
         rows = jnp.concatenate([query[base + b : base + b + 1] for b, _ in place_of], axis=0)
         wide = [
@@ -234,14 +243,27 @@
         scores = scores + decay[base : base + batches].reshape(per_group, -1)
         top = jnp.max(scores, axis=1, keepdims=True)
         short = jnp.exp(scores - top).astype(BF16).astype(F32)
-        total = jnp.sum(short, axis=1, keepdims=True)
+        return top, short, jnp.sum(short, axis=1, keepdims=True)
+
+    ahead = [weigh(group) for group in range(AHEAD)]
+    for group in range(groups):
+        base = group * batches
+        if group + AHEAD < groups:
+            ahead.append(weigh(group + AHEAD))
+        top, short, total = ahead[group]
+        for row in range(per_group):
+            wide = jnp.broadcast_to(short[row : row + 1], (8, short.shape[1]))
+            spread[group, row] = wide.astype(BF16)
         for row, (b, h) in enumerate(place_of):
-            mixed = jnp.zeros((HEAD_LANES, LANES), F32)
-            for place in range(0, short.shape[1], LANES):
-                value = values[
-                    group, row * HEAD_LANES : (row + 1) * HEAD_LANES, place : place + LANES
-                ]
-                mixed = mixed + value.astype(F32) * short[row : row + 1, place : place + LANES]
+            pieces = []
+            for first in range(row * HEAD_LANES, (row + 1) * HEAD_LANES, 8):
+                mixed = jnp.zeros((8, WIDE), F32)
+                for place in range(0, short.shape[1], WIDE):
+                    value = values[group, first : first + 8, place : place + WIDE]
+                    weight = spread[group, row, :, place : place + WIDE]
+                    mixed = mixed + value.astype(F32) * weight.astype(F32)
+                pieces.append(mixed[:, :LANES] + mixed[:, LANES:])
+            mixed = jnp.concatenate(pieces, axis=0)
             summed = jnp.sum(mixed, axis=1, keepdims=True)
             columns = jnp.where(column == h * batch + base + b, summed, columns)
         stats = jnp.where(tile_lane == group, top, stats)
@@ -341,10 +363,23 @@
     short[short.shape[0] - PACK :, :] = tail.astype(BF16)
 
 
+def down_columns(tp, core, active, down_weight, out):
+    def columns(pair):
+        low = pl.multiple_of((2 * pair + core) * LANES, LANES)
+        return down_weight[:, pl.ds(low, LANES)]
+
+    step = 2 if tp % 4 == 0 else 1
+    for pair in range(0, tp // 2, step):
+        weight = jnp.concatenate([columns(pair + index) for index in range(step)], axis=1)
+        product = dot(active, weight)
+        for index in range(step):
+            out[pair + index] = product[:, index * LANES : (index + 1) * LANES]
+
+
 def down_kernel(tp, size, count, *refs):
     full, short = refs[0], refs[1]
     others = refs[2 : 1 + count]
-    down_weight, keep, send, shares = refs[1 + count :]
+    down_weight, hidden, send = refs[1 + count :]
     batch, width = full.shape
     height = width // LANES * batch
     tail = short[height:, :].astype(F32)
@@ -361,13 +396,13 @@
             total = total + ref[block * batch : (block + 1) * batch, :].astype(F32)
         active = jnp.maximum(total * inverse, 0.0)
         pieces.append((active * active).astype(BF16))
-    product = dot(jnp.concatenate(pieces, axis=1), down_weight[...])
-    for block in range(tp):
-        shares[block] = product[:, block * LANES : (block + 1) * LANES]
-    core = lax.rem(lax.axis_index("tp"), 2)
-    for pair in range(tp // 2):
-        keep[pair] = shares[2 * pair + core]
-        send[pair] = shares[2 * pair + 1 - core]
+    active = jnp.concatenate(pieces, axis=1)
+    hidden[...] = active
+    down_columns(tp, 1 - lax.rem(lax.axis_index("tp"), 2), active, down_weight, send)
+
+
+def keep_kernel(tp, hidden, down_weight, keep):
+    down_columns(tp, lax.rem(lax.axis_index("tp"), 2), hidden[...], down_weight, keep)
 
 
 def split_kernel(pairs, keep, other, *refs):
@@ -444,7 +479,13 @@
         fan_kernel,
         [shape_of((count, batch, piece_width), BF16)],
         (stream,),
+    )
+    (fanned,) = kernel_call(
+        hold_kernel,
+        [shape_of((count, batch, piece_width), BF16)],
+        (fanned,),
         cost=pl.CostEstimate(flops=40_000_000_000, bytes_accessed=0, transcendentals=0),
+        aliases={0: 0},
     )
     blocks = lax.all_to_all(fanned, ("kv", "tp"), 0, 0)
     keys = jnp.swapaxes(key_cache, 2, 3).reshape(groups, depth, places)
@@ -467,6 +508,7 @@
             values,
             past_decay,
         ),
+        scratch=[pltpu.VMEM((groups, 8, 8, places), BF16)],
     )
     newest, owns = kernel_call(
         newest_kernel,
@@ -504,11 +546,15 @@
         scratch=[pltpu.VMEM((tp, batch, LANES), F32), pltpu.VMEM((batch, block_width), BF16)],
     )
     others = [trade(short, step) for step in range(1, kv)]
-    keep, send = kernel_call(
+    hidden, send = kernel_call(
         functools.partial(down_kernel, tp, size, kv),
-        [shape_of((pairs, batch, LANES), F32)] * 2,
+        [shape_of((batch, width), BF16), shape_of((pairs, batch, LANES), F32)],
         (full, short, *others, down_weight),
-        scratch=[pltpu.VMEM((tp, batch, LANES), F32)],
+    )
+    (keep,) = kernel_call(
+        functools.partial(keep_kernel, tp),
+        [shape_of((pairs, batch, LANES), F32)],
+        (hidden, down_weight),
     )
     *shares, own = kernel_call(
         functools.partial(split_kernel, pairs),

time: 56.8 us -> 55.7 us (0.981)
  waiting for transfers between devices: 17.3 us -> 16.6 us
    ppermute x2, waiting for transfers between devices: 2.57 us -> 1.84 us  [swap(): return lax.ppermute(array, 'tp', [(i, i ^ 1) for i in range(tp)])]
    pallas_call x9 -> x11, Pallas kernels: 6.44 us -> 6.21 us  [kernel_call(): pl.pallas_call(body, out_shape=tuple(out_shapes), in_specs=[pl.BlockSpec(...]
  transfers between devices with their start and end apart: 14 -> 14, of which waited for: 11 -> 11; matrix products, arithmetic and copies ran while one was open for 0% -> 0% of each run, Pallas kernels for 1% -> 2%
where the time goes in v3:
time: 55.7 us; the launch traced here: 55.5 us
  blocking collectives  17.1 us (31%)
  waiting for transfers between devices  16.6 us (30%)
  starting transfers between devices  14.6 us (26%)
  Pallas kernels  6.21 us (11%)
  local copies, waits for them, and re-layouts  0.8 us (1%)
    all_to_all x1, blocking collectives, shards(): blocks = lax.all_to_all(fanned, ('kv', 'tp'), 0, 0)  17.1 us
    ppermute x6, waiting for transfers between devices, trade(): return lax.ppermute(array, 'kv', [(i, i ^ step) for i in range(kv)])  8.14 us
    ppermute x6, starting transfers between devices, turn(): lax.ppermute(array, 'tp', [(i, (i + 2 * step) % tp) for i in range(tp)])  7.41 us
    ppermute x6, starting transfers between devices, trade(): return lax.ppermute(array, 'kv', [(i, i ^ step) for i in range(kv)])  7.07 us
    ppermute x6, waiting for transfers between devices, turn(): lax.ppermute(array, 'tp', [(i, (i + 2 * step) % tp) for i in range(tp)])  6.6 us
    pallas_call x11, Pallas kernels, kernel_call(): pl.pallas_call(body, out_shape=tuple(out_shapes), in_specs=[pl.BlockSpec(...  6.21 us
    ppermute x2, waiting for transfers between devices, swap(): return lax.ppermute(array, 'tp', [(i, i ^ 1) for i in range(tp)])  1.84 us
  transfers between devices with their start and end apart: 14, of which 11 were waited for; matrix products, arithmetic and copies ran while one was open for 0% of the time, Pallas kernels for 2%

profile of v3, /device:TPU:0, one launch (start us, length us, event | category | flops | bytes accessed | tf_op | source)
XLA Modules:
  0.0 55.5 jit_solution(10782125999192240731)
XLA Ops:
  0.0 0.7 %copy-done.12 = bf16[32,128]{1,0:T(8,128)(2,1)S(1)} copy-done((bf16[32,128]{1,0:T(8,128)(2,1)S(1)}, bf16[32,128]{1,0:T(8,128)(2,1)}, u32[]{:S(2)}) %copy-start.12) | copy-done | bytes 8216
  0.8 17.1 %all_to_all.5.blocks = bf16[32,32,128]{2,1,0:T(8,128)(2,1)S(1)} all-to-all(bf16[32,32,128]{2,1,0:T(8,128)(2,1)S(1)} %shard_map.137), channel_id=1, replica_groups=mesh['kv'=4,'tp'=8] {'kv','tp'}, dimensions={0} | all-to-all | bytes 524288 | tf_op jit(solution)/shard_map/all_to_all | solution.py:490
  18.1 2.5 %shard_map.138 = (f32[40,128]{1,0:T(8,128)S(1)}, bf16[32,4096]{1,0:T(8,128)(2,1)S(1)}, bf16[32,128]{1,0:T(8,128)(2,1)S(1)}) custom-call(bf16[32,32,128]{2,1,0:T(8,128)(2,1)S(1)} %all_to_all.5.blocks, f32[32,128]{1,0:T(8,128)S(1)} %bitcast.13, bf16[4096,128]{1,0:T(8,128)(2,1)S(1)} %copy-done.4, bf16[16,4096]{1,0:T(8,128)(2,1)S(1)} %bitcast.12, ...), custom_call_target="tpu_custom_call" | custom-call | tf_op jit(solution)/shard_map/pallas_call | solution.py:156
  20.6 1.2 %collective-permute-start.2 = (f32[40,128]{1,0:T(8,128)S(1)}, f32[40,128]{1,0:T(8,128)S(1)}, u32[]{:S(2)}, u32[]{:S(2)}) collective-permute-start(f32[40,128]{1,0:T(8,128)S(1)} %get-tuple-element.21.refs_0_), channel_id=1, source_target_pairs={{0,24},{8,16},{16,8},{24,0},{1,25},{9,17},{17,9},{25,1},{2,26},{10... | collective-permute-start | bytes 61448 | tf_op jit(solution)/shard_map/ppermute | solution.py:519
  21.8 1.2 %collective-permute-start.1 = (f32[40,128]{1,0:T(8,128)S(1)}, f32[40,128]{1,0:T(8,128)S(1)}, u32[]{:S(2)}, u32[]{:S(2)}) collective-permute-start(f32[40,128]{1,0:T(8,128)S(1)} %get-tuple-element.21.refs_0_), channel_id=1, source_target_pairs={{0,16},{8,24},{16,0},{24,8},{1,17},{9,25},{17,1},{25,9},{2,18},{10... | collective-permute-start | bytes 61448 | tf_op jit(solution)/shard_map/ppermute | solution.py:519
  22.9 1.2 %collective-permute-start = (f32[40,128]{1,0:T(8,128)S(1)}, f32[40,128]{1,0:T(8,128)S(1)}, u32[]{:S(2)}, u32[]{:S(2)}) collective-permute-start(f32[40,128]{1,0:T(8,128)S(1)} %get-tuple-element.21.refs_0_), channel_id=1, source_target_pairs={{0,8},{8,0},{16,24},{24,16},{1,9},{9,1},{17,25},{25,17},{2,10},{10... | collective-permute-start | bytes 61448 | tf_op jit(solution)/shard_map/ppermute | solution.py:519
  24.5 0.8 %collective-permute-done.2.refs_3_ = f32[40,128]{1,0:T(8,128)S(1)} collective-permute-done((f32[40,128]{1,0:T(8,128)S(1)}, f32[40,128]{1,0:T(8,128)S(1)}, u32[]{:S(2)}, u32[]{:S(2)}) %collective-permute-start.2) | collective-permute-done | bytes 20512 | tf_op jit(solution)/shard_map/ppermute | solution.py:519
  25.6 1.2 %collective-permute-done.refs_1_ = f32[40,128]{1,0:T(8,128)S(1)} collective-permute-done((f32[40,128]{1,0:T(8,128)S(1)}, f32[40,128]{1,0:T(8,128)S(1)}, u32[]{:S(2)}, u32[]{:S(2)}) %collective-permute-start) | collective-permute-done | bytes 20512 | tf_op jit(solution)/shard_map/ppermute | solution.py:519
  27.0 1.4 %collective-permute-start.5 = (bf16[32,1024]{1,0:T(8,128)(2,1)S(1)}, bf16[32,1024]{1,0:T(8,128)(2,1)S(1)}, u32[]{:S(2)}, u32[]{:S(2)}) collective-permute-start(bf16[32,1024]{1,0:T(8,128)(2,1)S(1)} %get-tuple-element.27), channel_id=1, source_target_pairs={{0,6},{1,7},{2,0},{3,1},{4,2},{5,3},{6,4},{7,5},{8,14},{9,15},{10,... | collective-permute-start | bytes 196616 | tf_op jit(solution)/shard_map/ppermute | solution.py:522
  28.4 1.8 %collective-permute-start.3 = (bf16[32,1024]{1,0:T(8,128)(2,1)S(1)}, bf16[32,1024]{1,0:T(8,128)(2,1)S(1)}, u32[]{:S(2)}, u32[]{:S(2)}) collective-permute-start(bf16[32,1024]{1,0:T(8,128)(2,1)S(1)} %get-tuple-element.27), channel_id=1, source_target_pairs={{0,2},{1,3},{2,4},{3,5},{4,6},{5,7},{6,0},{7,1},{8,10},{9,11},{10,... | collective-permute-start | bytes 196616 | tf_op jit(solution)/shard_map/ppermute | solution.py:522
  30.3 1.4 %collective-permute-done.5.refs_3_ = bf16[32,1024]{1,0:T(8,128)(2,1)S(1)} collective-permute-done((bf16[32,1024]{1,0:T(8,128)(2,1)S(1)}, bf16[32,1024]{1,0:T(8,128)(2,1)S(1)}, u32[]{:S(2)}, u32[]{:S(2)}) %collective-permute-start.5) | collective-permute-done | bytes 65568 | tf_op jit(solution)/shard_map/ppermute | solution.py:522
  31.6 3.4 %collective-permute-done.4.refs_2_ = bf16[32,1024]{1,0:T(8,128)(2,1)S(1)} collective-permute-done((bf16[32,1024]{1,0:T(8,128)(2,1)S(1)}, bf16[32,1024]{1,0:T(8,128)(2,1)S(1)}, u32[]{:S(2)}, u32[]{:S(2)}) %collective-permute-start.4) | collective-permute-done | bytes 65568 | tf_op jit(solution)/shard_map/ppermute | solution.py:522
  35.1 1.3 %collective-permute-done.6.two = f32[32,1024]{1,0:T(8,128)S(1)} collective-permute-done((f32[32,1024]{1,0:T(8,128)S(1)}, f32[32,1024]{1,0:T(8,128)S(1)}, u32[]{:S(2)}, u32[]{:S(2)}) %collective-permute-start.6) | collective-permute-done | bytes 131104 | tf_op jit(solution)/shard_map/ppermute | solution.py:525
  36.4 0.8 %shard_map.142 = (bf16[528,128]{1,0:T(8,128)(2,1)S(1)}, f32[32,2048]{1,0:T(8,128)S(1)}, f32[32,128]{1,0:T(8,128)S(1)}) custom-call(f32[32,1024]{1,0:T(8,128)S(1)} %shard_map.141.one, f32[32,1024]{1,0:T(8,128)S(1)} %collective-permute-done.6.two, bf16[32,32,128]{2,1,0:T(8,128)(2,1)S(1)} %all_to_all.5.blocks, f32[32,128]{1,0:T(8,128)S(1)} %bitcast.14, ...), custom_call_target="tpu_custom_call" | custom-call | tf_op jit(solution)/shard_map/pallas_call | solution.py:156
  37.2 1.9 %collective-permute-start.9 = (bf16[528,128]{1,0:T(8,128)(2,1)S(1)}, bf16[528,128]{1,0:T(8,128)(2,1)S(1)}, u32[]{:S(2)}, u32[]{:S(2)}) collective-permute-start(bf16[528,128]{1,0:T(8,128)(2,1)S(1)} %get-tuple-element.30.refs_1_), channel_id=1, source_target_pairs={{0,24},{8,16},{16,8},{24,0},{1,25},{9,17},{17,9},{25,1},{2,26},{10... | collective-permute-start | bytes 405512 | tf_op jit(solution)/shard_map/ppermute | solution.py:519
  39.2 1.2 %collective-permute-start.8 = (bf16[528,128]{1,0:T(8,128)(2,1)S(1)}, bf16[528,128]{1,0:T(8,128)(2,1)S(1)}, u32[]{:S(2)}, u32[]{:S(2)}) collective-permute-start(bf16[528,128]{1,0:T(8,128)(2,1)S(1)} %get-tuple-element.30.refs_1_), channel_id=1, source_target_pairs={{0,16},{8,24},{16,0},{24,8},{1,17},{9,25},{17,1},{25,9},{2,18},{10... | collective-permute-start | bytes 405512 | tf_op jit(solution)/shard_map/ppermute | solution.py:519
  40.7 3.9 %collective-permute-done.9.refs_4_ = bf16[528,128]{1,0:T(8,128)(2,1)S(1)} collective-permute-done((bf16[528,128]{1,0:T(8,128)(2,1)S(1)}, bf16[528,128]{1,0:T(8,128)(2,1)S(1)}, u32[]{:S(2)}, u32[]{:S(2)}) %collective-permute-start.9) | collective-permute-done | bytes 135200 | tf_op jit(solution)/shard_map/ppermute | solution.py:519
  44.6 2.1 %collective-permute-done.8.refs_3_ = bf16[528,128]{1,0:T(8,128)(2,1)S(1)} collective-permute-done((bf16[528,128]{1,0:T(8,128)(2,1)S(1)}, bf16[528,128]{1,0:T(8,128)(2,1)S(1)}, u32[]{:S(2)}, u32[]{:S(2)}) %collective-permute-start.8) | collective-permute-done | bytes 135200 | tf_op jit(solution)/shard_map/ppermute | solution.py:519
  46.7 0.8 %shard_map.143 = (bf16[32,2048]{1,0:T(8,128)(2,1)S(1)}, f32[4,32,128]{2,1,0:T(8,128)S(1)}) custom-call(f32[32,2048]{1,0:T(8,128)S(1)} %get-tuple-element.29.refs_0_, bf16[528,128]{1,0:T(8,128)(2,1)S(1)} %get-tuple-element.30.refs_1_, bf16[528,128]{1,0:T(8,128)(2,1)S(1)} %collective-permute-done.7.refs_2_, ...), custom_call_target="tpu_custom_call" | custom-call | tf_op jit(solution)/shard_map/pallas_call | solution.py:156
  47.5 0.7 %shard_map.144.keep = f32[4,32,128]{2,1,0:T(8,128)S(1)} custom-call(bf16[32,2048]{1,0:T(8,128)(2,1)S(1)} %get-tuple-element.31.hidden, bf16[2048,1024]{1,0:T(8,128)(2,1)S(1)} %copy-done), custom_call_target="tpu_custom_call" | custom-call | tf_op jit(solution)/shard_map/pallas_call | solution.py:156
  48.9 2.0 %collective-permute-start.12 = (bf16[32,128]{1,0:T(8,128)(2,1)S(1)}, bf16[32,128]{1,0:T(8,128)(2,1)S(1)}, u32[]{:S(2)}, u32[]{:S(2)}) collective-permute-start(bf16[32,128]{1,0:T(8,128)(2,1)S(1)} %get-tuple-element.35), channel_id=1, source_target_pairs={{0,4},{1,5},{2,6},{3,7},{4,0},{5,1},{6,2},{7,3},{8,12},{9,13},{10,... | collective-permute-start | bytes 24584 | tf_op jit(solution)/shard_map/ppermute | solution.py:522
  50.9 2.1 %collective-permute-start.13 = (bf16[32,128]{1,0:T(8,128)(2,1)S(1)}, bf16[32,128]{1,0:T(8,128)(2,1)S(1)}, u32[]{:S(2)}, u32[]{:S(2)}) collective-permute-start(bf16[32,128]{1,0:T(8,128)(2,1)S(1)} %get-tuple-element.36), channel_id=1, source_target_pairs={{0,6},{1,7},{2,0},{3,1},{4,2},{5,3},{6,4},{7,5},{8,14},{9,15},{10,... | collective-permute-start | bytes 24584 | tf_op jit(solution)/shard_map/ppermute | solution.py:522
  53.0 1.3 %collective-permute-done.11.refs_2_ = bf16[32,128]{1,0:T(8,128)(2,1)S(1)} collective-permute-done((bf16[32,128]{1,0:T(8,128)(2,1)S(1)}, bf16[32,128]{1,0:T(8,128)(2,1)S(1)}, u32[]{:S(2)}, u32[]{:S(2)}) %collective-permute-start.11) | collective-permute-done | bytes 8224 | tf_op jit(solution)/shard_map/ppermute | solution.py:522
  54.9 0.6 %shard_map.146 = bf16[32,128]{1,0:T(8,128)(2,1)} custom-call(f32[32,128]{1,0:T(8,128)S(1)} %get-tuple-element.28.refs_0_, f32[32,128]{1,0:T(8,128)S(1)} %get-tuple-element.33.refs_1_, bf16[32,128]{1,0:T(8,128)(2,1)S(1)} %collective-permute-done.11.refs_2_, bf16[32,128]{1,0:T(8,128)(2,1)S(1)} %collective-permute-done.12.refs_3_, ...), custom_call_target="tpu_custom_call" | custom-call | tf_op jit(solution)/shard_map/pallas_call | solution.py:156
  (44 shorter events, 2.7 us)
Async XLA Ops:
  0.7 17.2 %copy-start.1 = (bf16[32,2,1024,64]{2,3,1,0:T(8,128)(2,1)S(1)}, bf16[32,2,1024,64]{2,3,1,0:T(8,128)(2,1)}, u32[]{:S(2)}) copy-start(bf16[32,2,1024,64]{2,3,1,0:T(8,128)(2,1)} %param.21) | copy-start | bytes 25165828
  0.7 17.2 %copy-start.2 = (bf16[32,2,1024,64]{2,3,1,0:T(8,128)(2,1)S(1)}, bf16[32,2,1024,64]{2,3,1,0:T(8,128)(2,1)}, u32[]{:S(2)}) copy-start(bf16[32,2,1024,64]{2,3,1,0:T(8,128)(2,1)} %param.22) | copy-start | bytes 25165828
  0.8 17.2 %copy-start.4 = (bf16[4096,128]{1,0:T(8,128)(2,1)S(1)}, bf16[4096,128]{1,0:T(8,128)(2,1)}, u32[]{:S(2)}) copy-start(bf16[4096,128]{1,0:T(8,128)(2,1)} %query_weight.1) | copy-start | bytes 3145732
  0.8 17.2 %copy-start.7 = (f32[32,2,1024]{2,1,0:T(2,128)S(1)}, f32[32,2,1024]{2,1,0:T(2,128)}, u32[]{:S(2)}) copy-start(f32[32,2,1024]{2,1,0:T(2,128)} %decay.1) | copy-start | bytes 786436
  0.8 17.2 %copy-start.9 = (bf16[4096,16]{0,1:T(8,128)(2,1)S(1)}, bf16[4096,16]{0,1:T(8,128)(2,1)}, u32[]{:S(2)}) copy-start(bf16[4096,16]{0,1:T(8,128)(2,1)} %param.19) | copy-start | bytes 393220
  0.8 17.2 %copy-start.10 = (f32[4096]{0:T(1024)S(1)}, f32[4096]{0:T(1024)}, u32[]{:S(2)}) copy-start(f32[4096]{0:T(1024)} %param.15) | copy-start | bytes 49156
  0.8 17.2 %copy-start.13 = (f32[16]{0:T(128)S(1)}, f32[16]{0:T(128)}, u32[]{:S(2)}) copy-start(f32[16]{0:T(128)} %param.20) | copy-start | bytes 196
  18.1 18.4 %copy-start.3 = (bf16[1024,2048]{1,0:T(8,128)(2,1)S(1)}, bf16[1024,2048]{1,0:T(8,128)(2,1)}, u32[]{:S(2)}) copy-start(bf16[1024,2048]{1,0:T(8,128)(2,1)} %up_weight.1) | copy-start | bytes 12582916
  18.1 18.4 %copy-start.11 = (f32[4096]{0:T(1024)S(1)}, f32[4096]{0:T(1024)}, u32[]{:S(2)}) copy-start(f32[4096]{0:T(1024)} %param.25) | copy-start | bytes 49156
  20.5 26.2 %copy-start = (bf16[2048,1024]{1,0:T(8,128)(2,1)S(1)}, bf16[2048,1024]{1,0:T(8,128)(2,1)}, u32[]{:S(2)}) copy-start(bf16[2048,1024]{1,0:T(8,128)(2,1)} %down_weight.1) | copy-start | bytes 12582916
  20.6 4.7 %collective-permute-start.2 = (f32[40,128]{1,0:T(8,128)S(1)}, f32[40,128]{1,0:T(8,128)S(1)}, u32[]{:S(2)}, u32[]{:S(2)}) collective-permute-start(f32[40,128]{1,0:T(8,128)S(1)} %get-tuple-element.21.refs_0_), channel_id=1, source_target_pairs={{0,24},{8,16},{16,8},{24,0},{1,25},{9,17},{17,9},{25,1},{2,26},{10... | collective-permute-start | bytes 61448 | tf_op jit(solution)/shard_map/ppermute | solution.py:519
  21.8 3.8 %collective-permute-start.1 = (f32[40,128]{1,0:T(8,128)S(1)}, f32[40,128]{1,0:T(8,128)S(1)}, u32[]{:S(2)}, u32[]{:S(2)}) collective-permute-start(f32[40,128]{1,0:T(8,128)S(1)} %get-tuple-element.21.refs_0_), channel_id=1, source_target_pairs={{0,16},{8,24},{16,0},{24,8},{1,17},{9,25},{17,1},{25,9},{2,18},{10... | collective-permute-start | bytes 61448 | tf_op jit(solution)/shard_map/ppermute | solution.py:519
  22.9 3.8 %collective-permute-start = (f32[40,128]{1,0:T(8,128)S(1)}, f32[40,128]{1,0:T(8,128)S(1)}, u32[]{:S(2)}, u32[]{:S(2)}) collective-permute-start(f32[40,128]{1,0:T(8,128)S(1)} %get-tuple-element.21.refs_0_), channel_id=1, source_target_pairs={{0,8},{8,0},{16,24},{24,16},{1,9},{9,1},{17,25},{25,17},{2,10},{10... | collective-permute-start | bytes 61448 | tf_op jit(solution)/shard_map/ppermute | solution.py:519
  27.0 4.6 %collective-permute-start.5 = (bf16[32,1024]{1,0:T(8,128)(2,1)S(1)}, bf16[32,1024]{1,0:T(8,128)(2,1)S(1)}, u32[]{:S(2)}, u32[]{:S(2)}) collective-permute-start(bf16[32,1024]{1,0:T(8,128)(2,1)S(1)} %get-tuple-element.27), channel_id=1, source_target_pairs={{0,6},{1,7},{2,0},{3,1},{4,2},{5,3},{6,4},{7,5},{8,14},{9,15},{10,... | collective-permute-start | bytes 196616 | tf_op jit(solution)/shard_map/ppermute | solution.py:522
  28.4 6.6 %collective-permute-start.4 = (bf16[32,1024]{1,0:T(8,128)(2,1)S(1)}, bf16[32,1024]{1,0:T(8,128)(2,1)S(1)}, u32[]{:S(2)}, u32[]{:S(2)}) collective-permute-start(bf16[32,1024]{1,0:T(8,128)(2,1)S(1)} %get-tuple-element.27), channel_id=1, source_target_pairs={{0,4},{1,5},{2,6},{3,7},{4,0},{5,1},{6,2},{7,3},{8,12},{9,13},{10,... | collective-permute-start | bytes 196616 | tf_op jit(solution)/shard_map/ppermute | solution.py:522
  28.4 6.5 %collective-permute-start.3 = (bf16[32,1024]{1,0:T(8,128)(2,1)S(1)}, bf16[32,1024]{1,0:T(8,128)(2,1)S(1)}, u32[]{:S(2)}, u32[]{:S(2)}) collective-permute-start(bf16[32,1024]{1,0:T(8,128)(2,1)S(1)} %get-tuple-element.27), channel_id=1, source_target_pairs={{0,2},{1,3},{2,4},{3,5},{4,6},{5,7},{6,0},{7,1},{8,10},{9,11},{10,... | collective-permute-start | bytes 196616 | tf_op jit(solution)/shard_map/ppermute | solution.py:522
  35.0 1.4 %collective-permute-start.6 = (f32[32,1024]{1,0:T(8,128)S(1)}, f32[32,1024]{1,0:T(8,128)S(1)}, u32[]{:S(2)}, u32[]{:S(2)}) collective-permute-start(f32[32,1024]{1,0:T(8,128)S(1)} %shard_map.141.one), channel_id=1, source_target_pairs={{0,1},{1,0},{2,3},{3,2},{4,5},{5,4},{6,7},{7,6},{8,9},{9,8},{10,11... | collective-permute-start | bytes 393224 | tf_op jit(solution)/shard_map/ppermute | solution.py:525
  37.2 7.4 %collective-permute-start.9 = (bf16[528,128]{1,0:T(8,128)(2,1)S(1)}, bf16[528,128]{1,0:T(8,128)(2,1)S(1)}, u32[]{:S(2)}, u32[]{:S(2)}) collective-permute-start(bf16[528,128]{1,0:T(8,128)(2,1)S(1)} %get-tuple-element.30.refs_1_), channel_id=1, source_target_pairs={{0,24},{8,16},{16,8},{24,0},{1,25},{9,17},{17,9},{25,1},{2,26},{10... | collective-permute-start | bytes 405512 | tf_op jit(solution)/shard_map/ppermute | solution.py:519
  39.2 7.5 %collective-permute-start.8 = (bf16[528,128]{1,0:T(8,128)(2,1)S(1)}, bf16[528,128]{1,0:T(8,128)(2,1)S(1)}, u32[]{:S(2)}, u32[]{:S(2)}) collective-permute-start(bf16[528,128]{1,0:T(8,128)(2,1)S(1)} %get-tuple-element.30.refs_1_), channel_id=1, source_target_pairs={{0,16},{8,24},{16,0},{24,8},{1,17},{9,25},{17,1},{25,9},{2,18},{10... | collective-permute-start | bytes 405512 | tf_op jit(solution)/shard_map/ppermute | solution.py:519
  40.4 6.3 %collective-permute-start.7 = (bf16[528,128]{1,0:T(8,128)(2,1)S(1)}, bf16[528,128]{1,0:T(8,128)(2,1)S(1)}, u32[]{:S(2)}, u32[]{:S(2)}) collective-permute-start(bf16[528,128]{1,0:T(8,128)(2,1)S(1)} %get-tuple-element.30.refs_1_), channel_id=1, source_target_pairs={{0,8},{8,0},{16,24},{24,16},{1,9},{9,1},{17,25},{25,17},{2,10},{10... | collective-permute-start | bytes 405512 | tf_op jit(solution)/shard_map/ppermute | solution.py:519
  47.5 1.3 %collective-permute-start.10 = (f32[4,32,128]{2,1,0:T(8,128)S(1)}, f32[4,32,128]{2,1,0:T(8,128)S(1)}, u32[]{:S(2)}, u32[]{:S(2)}) collective-permute-start(f32[4,32,128]{2,1,0:T(8,128)S(1)} %get-tuple-element.32), channel_id=1, source_target_pairs={{0,1},{1,0},{2,3},{3,2},{4,5},{5,4},{6,7},{7,6},{8,9},{9,8},{10,11... | collective-permute-start | bytes 196616 | tf_op jit(solution)/shard_map/ppermute | solution.py:525
  48.8 5.5 %collective-permute-start.11 = (bf16[32,128]{1,0:T(8,128)(2,1)S(1)}, bf16[32,128]{1,0:T(8,128)(2,1)S(1)}, u32[]{:S(2)}, u32[]{:S(2)}) collective-permute-start(bf16[32,128]{1,0:T(8,128)(2,1)S(1)} %get-tuple-element.34), channel_id=1, source_target_pairs={{0,2},{1,3},{2,4},{3,5},{4,6},{5,7},{6,0},{7,1},{8,10},{9,11},{10,... | collective-permute-start | bytes 24584 | tf_op jit(solution)/shard_map/ppermute | solution.py:522
  48.9 5.4 %collective-permute-start.12 = (bf16[32,128]{1,0:T(8,128)(2,1)S(1)}, bf16[32,128]{1,0:T(8,128)(2,1)S(1)}, u32[]{:S(2)}, u32[]{:S(2)}) collective-permute-start(bf16[32,128]{1,0:T(8,128)(2,1)S(1)} %get-tuple-element.35), channel_id=1, source_target_pairs={{0,4},{1,5},{2,6},{3,7},{4,0},{5,1},{6,2},{7,3},{8,12},{9,13},{10,... | collective-permute-start | bytes 24584 | tf_op jit(solution)/shard_map/ppermute | solution.py:522
  50.9 4.0 %collective-permute-start.13 = (bf16[32,128]{1,0:T(8,128)(2,1)S(1)}, bf16[32,128]{1,0:T(8,128)(2,1)S(1)}, u32[]{:S(2)}, u32[]{:S(2)}) collective-permute-start(bf16[32,128]{1,0:T(8,128)(2,1)S(1)} %get-tuple-element.36), channel_id=1, source_target_pairs={{0,6},{1,7},{2,0},{3,1},{4,2},{5,3},{6,4},{7,5},{8,14},{9,15},{10,... | collective-permute-start | bytes 24584 | tf_op jit(solution)/shard_map/ppermute | solution.py:522
  (4 other events, 21.6 us)

commit v4 on v3

--- a/solution.py
+++ b/solution.py
@@ -138,7 +138,7 @@
 HEAD_LANES = 64
 PACK = 16
 WIDE = 256
-AHEAD = 1
+AHEAD = 2
 F32 = jnp.float32
 BF16 = jnp.bfloat16
 CONTRACT_LAST = (((1,), (1,)), ((), ()))

time: 55.7 us -> 55.7 us (level)
  no operation moved by 1% of the time
where the time goes in v4:
time: 55.7 us; the launch traced here: 55.4 us
  blocking collectives  17.1 us (31%)
  waiting for transfers between devices  16.6 us (30%)
  starting transfers between devices  14.6 us (26%)
  Pallas kernels  6.18 us (11%)
  local copies, waits for them, and re-layouts  0.8 us (1%)
    all_to_all x1, blocking collectives, shards(): blocks = lax.all_to_all(fanned, ('kv', 'tp'), 0, 0)  17.1 us
    ppermute x6, waiting for transfers between devices, trade(): return lax.ppermute(array, 'kv', [(i, i ^ step) for i in range(kv)])  8.14 us
    ppermute x6, starting transfers between devices, turn(): lax.ppermute(array, 'tp', [(i, (i + 2 * step) % tp) for i in range(tp)])  7.4 us
    ppermute x6, starting transfers between devices, trade(): return lax.ppermute(array, 'kv', [(i, i ^ step) for i in range(kv)])  7.07 us
    ppermute x6, waiting for transfers between devices, turn(): lax.ppermute(array, 'tp', [(i, (i + 2 * step) % tp) for i in range(tp)])  6.6 us
    pallas_call x11, Pallas kernels, kernel_call(): pl.pallas_call(body, out_shape=tuple(out_shapes), in_specs=[pl.BlockSpec(...  6.18 us
    ppermute x2, waiting for transfers between devices, swap(): return lax.ppermute(array, 'tp', [(i, i ^ 1) for i in range(tp)])  1.84 us
  transfers between devices with their start and end apart: 14, of which 11 were waited for; matrix products, arithmetic and copies ran while one was open for 0% of the time, Pallas kernels for 2%

profile of v4, /device:TPU:0, one launch (start us, length us, event | category | flops | bytes accessed | tf_op | source)
XLA Modules:
  0.0 55.4 jit_solution(2675942178778541781)
XLA Ops:
  0.0 0.7 %copy-done.12 = bf16[32,128]{1,0:T(8,128)(2,1)S(1)} copy-done((bf16[32,128]{1,0:T(8,128)(2,1)S(1)}, bf16[32,128]{1,0:T(8,128)(2,1)}, u32[]{:S(2)}) %copy-start.12) | copy-done | bytes 8216
  0.8 17.1 %all_to_all.5.blocks = bf16[32,32,128]{2,1,0:T(8,128)(2,1)S(1)} all-to-all(bf16[32,32,128]{2,1,0:T(8,128)(2,1)S(1)} %shard_map.137), channel_id=1, replica_groups=mesh['kv'=4,'tp'=8] {'kv','tp'}, dimensions={0} | all-to-all | bytes 524288 | tf_op jit(solution)/shard_map/all_to_all | solution.py:490
  18.1 2.4 %shard_map.138 = (f32[40,128]{1,0:T(8,128)S(1)}, bf16[32,4096]{1,0:T(8,128)(2,1)S(1)}, bf16[32,128]{1,0:T(8,128)(2,1)S(1)}) custom-call(bf16[32,32,128]{2,1,0:T(8,128)(2,1)S(1)} %all_to_all.5.blocks, f32[32,128]{1,0:T(8,128)S(1)} %bitcast.13, bf16[4096,128]{1,0:T(8,128)(2,1)S(1)} %copy-done.4, bf16[16,4096]{1,0:T(8,128)(2,1)S(1)} %bitcast.12, ...), custom_call_target="tpu_custom_call" | custom-call | tf_op jit(solution)/shard_map/pallas_call | solution.py:156
  20.5 1.2 %collective-permute-start.2 = (f32[40,128]{1,0:T(8,128)S(1)}, f32[40,128]{1,0:T(8,128)S(1)}, u32[]{:S(2)}, u32[]{:S(2)}) collective-permute-start(f32[40,128]{1,0:T(8,128)S(1)} %get-tuple-element.21.refs_0_), channel_id=1, source_target_pairs={{0,24},{8,16},{16,8},{24,0},{1,25},{9,17},{17,9},{25,1},{2,26},{10... | collective-permute-start | bytes 61448 | tf_op jit(solution)/shard_map/ppermute | solution.py:519
  21.7 1.2 %collective-permute-start.1 = (f32[40,128]{1,0:T(8,128)S(1)}, f32[40,128]{1,0:T(8,128)S(1)}, u32[]{:S(2)}, u32[]{:S(2)}) collective-permute-start(f32[40,128]{1,0:T(8,128)S(1)} %get-tuple-element.21.refs_0_), channel_id=1, source_target_pairs={{0,16},{8,24},{16,0},{24,8},{1,17},{9,25},{17,1},{25,9},{2,18},{10... | collective-permute-start | bytes 61448 | tf_op jit(solution)/shard_map/ppermute | solution.py:519
  22.9 1.2 %collective-permute-start = (f32[40,128]{1,0:T(8,128)S(1)}, f32[40,128]{1,0:T(8,128)S(1)}, u32[]{:S(2)}, u32[]{:S(2)}) collective-permute-start(f32[40,128]{1,0:T(8,128)S(1)} %get-tuple-element.21.refs_0_), channel_id=1, source_target_pairs={{0,8},{8,0},{16,24},{24,16},{1,9},{9,1},{17,25},{25,17},{2,10},{10... | collective-permute-start | bytes 61448 | tf_op jit(solution)/shard_map/ppermute | solution.py:519
  24.5 0.8 %collective-permute-done.2.refs_3_ = f32[40,128]{1,0:T(8,128)S(1)} collective-permute-done((f32[40,128]{1,0:T(8,128)S(1)}, f32[40,128]{1,0:T(8,128)S(1)}, u32[]{:S(2)}, u32[]{:S(2)}) %collective-permute-start.2) | collective-permute-done | bytes 20512 | tf_op jit(solution)/shard_map/ppermute | solution.py:519
  25.5 1.2 %collective-permute-done.refs_1_ = f32[40,128]{1,0:T(8,128)S(1)} collective-permute-done((f32[40,128]{1,0:T(8,128)S(1)}, f32[40,128]{1,0:T(8,128)S(1)}, u32[]{:S(2)}, u32[]{:S(2)}) %collective-permute-start) | collective-permute-done | bytes 20512 | tf_op jit(solution)/shard_map/ppermute | solution.py:519
  27.0 1.4 %collective-permute-start.5 = (bf16[32,1024]{1,0:T(8,128)(2,1)S(1)}, bf16[32,1024]{1,0:T(8,128)(2,1)S(1)}, u32[]{:S(2)}, u32[]{:S(2)}) collective-permute-start(bf16[32,1024]{1,0:T(8,128)(2,1)S(1)} %get-tuple-element.27), channel_id=1, source_target_pairs={{0,6},{1,7},{2,0},{3,1},{4,2},{5,3},{6,4},{7,5},{8,14},{9,15},{10,... | collective-permute-start | bytes 196616 | tf_op jit(solution)/shard_map/ppermute | solution.py:522
  28.4 1.8 %collective-permute-start.3 = (bf16[32,1024]{1,0:T(8,128)(2,1)S(1)}, bf16[32,1024]{1,0:T(8,128)(2,1)S(1)}, u32[]{:S(2)}, u32[]{:S(2)}) collective-permute-start(bf16[32,1024]{1,0:T(8,128)(2,1)S(1)} %get-tuple-element.27), channel_id=1, source_target_pairs={{0,2},{1,3},{2,4},{3,5},{4,6},{5,7},{6,0},{7,1},{8,10},{9,11},{10,... | collective-permute-start | bytes 196616 | tf_op jit(solution)/shard_map/ppermute | solution.py:522
  30.2 1.4 %collective-permute-done.5.refs_3_ = bf16[32,1024]{1,0:T(8,128)(2,1)S(1)} collective-permute-done((bf16[32,1024]{1,0:T(8,128)(2,1)S(1)}, bf16[32,1024]{1,0:T(8,128)(2,1)S(1)}, u32[]{:S(2)}, u32[]{:S(2)}) %collective-permute-start.5) | collective-permute-done | bytes 65568 | tf_op jit(solution)/shard_map/ppermute | solution.py:522
  31.6 3.4 %collective-permute-done.4.refs_2_ = bf16[32,1024]{1,0:T(8,128)(2,1)S(1)} collective-permute-done((bf16[32,1024]{1,0:T(8,128)(2,1)S(1)}, bf16[32,1024]{1,0:T(8,128)(2,1)S(1)}, u32[]{:S(2)}, u32[]{:S(2)}) %collective-permute-start.4) | collective-permute-done | bytes 65568 | tf_op jit(solution)/shard_map/ppermute | solution.py:522
  35.0 1.3 %collective-permute-done.6.two = f32[32,1024]{1,0:T(8,128)S(1)} collective-permute-done((f32[32,1024]{1,0:T(8,128)S(1)}, f32[32,1024]{1,0:T(8,128)S(1)}, u32[]{:S(2)}, u32[]{:S(2)}) %collective-permute-start.6) | collective-permute-done | bytes 131104 | tf_op jit(solution)/shard_map/ppermute | solution.py:525
  36.4 0.8 %shard_map.142 = (bf16[528,128]{1,0:T(8,128)(2,1)S(1)}, f32[32,2048]{1,0:T(8,128)S(1)}, f32[32,128]{1,0:T(8,128)S(1)}) custom-call(f32[32,1024]{1,0:T(8,128)S(1)} %shard_map.141.one, f32[32,1024]{1,0:T(8,128)S(1)} %collective-permute-done.6.two, bf16[32,32,128]{2,1,0:T(8,128)(2,1)S(1)} %all_to_all.5.blocks, f32[32,128]{1,0:T(8,128)S(1)} %bitcast.14, ...), custom_call_target="tpu_custom_call" | custom-call | tf_op jit(solution)/shard_map/pallas_call | solution.py:156
  37.2 1.9 %collective-permute-start.9 = (bf16[528,128]{1,0:T(8,128)(2,1)S(1)}, bf16[528,128]{1,0:T(8,128)(2,1)S(1)}, u32[]{:S(2)}, u32[]{:S(2)}) collective-permute-start(bf16[528,128]{1,0:T(8,128)(2,1)S(1)} %get-tuple-element.30.refs_1_), channel_id=1, source_target_pairs={{0,24},{8,16},{16,8},{24,0},{1,25},{9,17},{17,9},{25,1},{2,26},{10... | collective-permute-start | bytes 405512 | tf_op jit(solution)/shard_map/ppermute | solution.py:519
  39.1 1.2 %collective-permute-start.8 = (bf16[528,128]{1,0:T(8,128)(2,1)S(1)}, bf16[528,128]{1,0:T(8,128)(2,1)S(1)}, u32[]{:S(2)}, u32[]{:S(2)}) collective-permute-start(bf16[528,128]{1,0:T(8,128)(2,1)S(1)} %get-tuple-element.30.refs_1_), channel_id=1, source_target_pairs={{0,16},{8,24},{16,0},{24,8},{1,17},{9,25},{17,1},{25,9},{2,18},{10... | collective-permute-start | bytes 405512 | tf_op jit(solution)/shard_map/ppermute | solution.py:519
  40.7 3.9 %collective-permute-done.9.refs_4_ = bf16[528,128]{1,0:T(8,128)(2,1)S(1)} collective-permute-done((bf16[528,128]{1,0:T(8,128)(2,1)S(1)}, bf16[528,128]{1,0:T(8,128)(2,1)S(1)}, u32[]{:S(2)}, u32[]{:S(2)}) %collective-permute-start.9) | collective-permute-done | bytes 135200 | tf_op jit(solution)/shard_map/ppermute | solution.py:519
  44.6 2.1 %collective-permute-done.8.refs_3_ = bf16[528,128]{1,0:T(8,128)(2,1)S(1)} collective-permute-done((bf16[528,128]{1,0:T(8,128)(2,1)S(1)}, bf16[528,128]{1,0:T(8,128)(2,1)S(1)}, u32[]{:S(2)}, u32[]{:S(2)}) %collective-permute-start.8) | collective-permute-done | bytes 135200 | tf_op jit(solution)/shard_map/ppermute | solution.py:519
  46.7 0.8 %shard_map.143 = (bf16[32,2048]{1,0:T(8,128)(2,1)S(1)}, f32[4,32,128]{2,1,0:T(8,128)S(1)}) custom-call(f32[32,2048]{1,0:T(8,128)S(1)} %get-tuple-element.29.refs_0_, bf16[528,128]{1,0:T(8,128)(2,1)S(1)} %get-tuple-element.30.refs_1_, bf16[528,128]{1,0:T(8,128)(2,1)S(1)} %collective-permute-done.7.refs_2_, ...), custom_call_target="tpu_custom_call" | custom-call | tf_op jit(solution)/shard_map/pallas_call | solution.py:156
  47.5 0.7 %shard_map.144.keep = f32[4,32,128]{2,1,0:T(8,128)S(1)} custom-call(bf16[32,2048]{1,0:T(8,128)(2,1)S(1)} %get-tuple-element.31.hidden, bf16[2048,1024]{1,0:T(8,128)(2,1)S(1)} %copy-done), custom_call_target="tpu_custom_call" | custom-call | tf_op jit(solution)/shard_map/pallas_call | solution.py:156
  48.8 2.0 %collective-permute-start.12 = (bf16[32,128]{1,0:T(8,128)(2,1)S(1)}, bf16[32,128]{1,0:T(8,128)(2,1)S(1)}, u32[]{:S(2)}, u32[]{:S(2)}) collective-permute-start(bf16[32,128]{1,0:T(8,128)(2,1)S(1)} %get-tuple-element.35), channel_id=1, source_target_pairs={{0,4},{1,5},{2,6},{3,7},{4,0},{5,1},{6,2},{7,3},{8,12},{9,13},{10,... | collective-permute-start | bytes 24584 | tf_op jit(solution)/shard_map/ppermute | solution.py:522
  50.9 2.1 %collective-permute-start.13 = (bf16[32,128]{1,0:T(8,128)(2,1)S(1)}, bf16[32,128]{1,0:T(8,128)(2,1)S(1)}, u32[]{:S(2)}, u32[]{:S(2)}) collective-permute-start(bf16[32,128]{1,0:T(8,128)(2,1)S(1)} %get-tuple-element.36), channel_id=1, source_target_pairs={{0,6},{1,7},{2,0},{3,1},{4,2},{5,3},{6,4},{7,5},{8,14},{9,15},{10,... | collective-permute-start | bytes 24584 | tf_op jit(solution)/shard_map/ppermute | solution.py:522
  53.0 1.3 %collective-permute-done.11.refs_2_ = bf16[32,128]{1,0:T(8,128)(2,1)S(1)} collective-permute-done((bf16[32,128]{1,0:T(8,128)(2,1)S(1)}, bf16[32,128]{1,0:T(8,128)(2,1)S(1)}, u32[]{:S(2)}, u32[]{:S(2)}) %collective-permute-start.11) | collective-permute-done | bytes 8224 | tf_op jit(solution)/shard_map/ppermute | solution.py:522
  54.8 0.6 %shard_map.146 = bf16[32,128]{1,0:T(8,128)(2,1)} custom-call(f32[32,128]{1,0:T(8,128)S(1)} %get-tuple-element.28.refs_0_, f32[32,128]{1,0:T(8,128)S(1)} %get-tuple-element.33.refs_1_, bf16[32,128]{1,0:T(8,128)(2,1)S(1)} %collective-permute-done.11.refs_2_, bf16[32,128]{1,0:T(8,128)(2,1)S(1)} %collective-permute-done.12.refs_3_, ...), custom_call_target="tpu_custom_call" | custom-call | tf_op jit(solution)/shard_map/pallas_call | solution.py:156
  (44 shorter events, 2.7 us)
Async XLA Ops:
  0.7 17.2 %copy-start.1 = (bf16[32,2,1024,64]{2,3,1,0:T(8,128)(2,1)S(1)}, bf16[32,2,1024,64]{2,3,1,0:T(8,128)(2,1)}, u32[]{:S(2)}) copy-start(bf16[32,2,1024,64]{2,3,1,0:T(8,128)(2,1)} %param.21) | copy-start | bytes 25165828
  0.7 17.2 %copy-start.2 = (bf16[32,2,1024,64]{2,3,1,0:T(8,128)(2,1)S(1)}, bf16[32,2,1024,64]{2,3,1,0:T(8,128)(2,1)}, u32[]{:S(2)}) copy-start(bf16[32,2,1024,64]{2,3,1,0:T(8,128)(2,1)} %param.22) | copy-start | bytes 25165828
  0.8 17.2 %copy-start.4 = (bf16[4096,128]{1,0:T(8,128)(2,1)S(1)}, bf16[4096,128]{1,0:T(8,128)(2,1)}, u32[]{:S(2)}) copy-start(bf16[4096,128]{1,0:T(8,128)(2,1)} %query_weight.1) | copy-start | bytes 3145732
  0.8 17.2 %copy-start.7 = (f32[32,2,1024]{2,1,0:T(2,128)S(1)}, f32[32,2,1024]{2,1,0:T(2,128)}, u32[]{:S(2)}) copy-start(f32[32,2,1024]{2,1,0:T(2,128)} %decay.1) | copy-start | bytes 786436
  0.8 17.2 %copy-start.9 = (bf16[4096,16]{0,1:T(8,128)(2,1)S(1)}, bf16[4096,16]{0,1:T(8,128)(2,1)}, u32[]{:S(2)}) copy-start(bf16[4096,16]{0,1:T(8,128)(2,1)} %param.19) | copy-start | bytes 393220
  0.8 17.2 %copy-start.10 = (f32[4096]{0:T(1024)S(1)}, f32[4096]{0:T(1024)}, u32[]{:S(2)}) copy-start(f32[4096]{0:T(1024)} %param.15) | copy-start | bytes 49156
  0.8 17.2 %copy-start.13 = (f32[16]{0:T(128)S(1)}, f32[16]{0:T(128)}, u32[]{:S(2)}) copy-start(f32[16]{0:T(128)} %param.20) | copy-start | bytes 196
  18.1 18.3 %copy-start.3 = (bf16[1024,2048]{1,0:T(8,128)(2,1)S(1)}, bf16[1024,2048]{1,0:T(8,128)(2,1)}, u32[]{:S(2)}) copy-start(bf16[1024,2048]{1,0:T(8,128)(2,1)} %up_weight.1) | copy-start | bytes 12582916
  18.1 18.3 %copy-start.11 = (f32[4096]{0:T(1024)S(1)}, f32[4096]{0:T(1024)}, u32[]{:S(2)}) copy-start(f32[4096]{0:T(1024)} %param.25) | copy-start | bytes 49156
  20.5 26.2 %copy-start = (bf16[2048,1024]{1,0:T(8,128)(2,1)S(1)}, bf16[2048,1024]{1,0:T(8,128)(2,1)}, u32[]{:S(2)}) copy-start(bf16[2048,1024]{1,0:T(8,128)(2,1)} %down_weight.1) | copy-start | bytes 12582916
  20.5 4.7 %collective-permute-start.2 = (f32[40,128]{1,0:T(8,128)S(1)}, f32[40,128]{1,0:T(8,128)S(1)}, u32[]{:S(2)}, u32[]{:S(2)}) collective-permute-start(f32[40,128]{1,0:T(8,128)S(1)} %get-tuple-element.21.refs_0_), channel_id=1, source_target_pairs={{0,24},{8,16},{16,8},{24,0},{1,25},{9,17},{17,9},{25,1},{2,26},{10... | collective-permute-start | bytes 61448 | tf_op jit(solution)/shard_map/ppermute | solution.py:519
  21.7 3.8 %collective-permute-start.1 = (f32[40,128]{1,0:T(8,128)S(1)}, f32[40,128]{1,0:T(8,128)S(1)}, u32[]{:S(2)}, u32[]{:S(2)}) collective-permute-start(f32[40,128]{1,0:T(8,128)S(1)} %get-tuple-element.21.refs_0_), channel_id=1, source_target_pairs={{0,16},{8,24},{16,0},{24,8},{1,17},{9,25},{17,1},{25,9},{2,18},{10... | collective-permute-start | bytes 61448 | tf_op jit(solution)/shard_map/ppermute | solution.py:519
  22.9 3.8 %collective-permute-start = (f32[40,128]{1,0:T(8,128)S(1)}, f32[40,128]{1,0:T(8,128)S(1)}, u32[]{:S(2)}, u32[]{:S(2)}) collective-permute-start(f32[40,128]{1,0:T(8,128)S(1)} %get-tuple-element.21.refs_0_), channel_id=1, source_target_pairs={{0,8},{8,0},{16,24},{24,16},{1,9},{9,1},{17,25},{25,17},{2,10},{10... | collective-permute-start | bytes 61448 | tf_op jit(solution)/shard_map/ppermute | solution.py:519
  27.0 4.6 %collective-permute-start.5 = (bf16[32,1024]{1,0:T(8,128)(2,1)S(1)}, bf16[32,1024]{1,0:T(8,128)(2,1)S(1)}, u32[]{:S(2)}, u32[]{:S(2)}) collective-permute-start(bf16[32,1024]{1,0:T(8,128)(2,1)S(1)} %get-tuple-element.27), channel_id=1, source_target_pairs={{0,6},{1,7},{2,0},{3,1},{4,2},{5,3},{6,4},{7,5},{8,14},{9,15},{10,... | collective-permute-start | bytes 196616 | tf_op jit(solution)/shard_map/ppermute | solution.py:522
  28.3 6.6 %collective-permute-start.4 = (bf16[32,1024]{1,0:T(8,128)(2,1)S(1)}, bf16[32,1024]{1,0:T(8,128)(2,1)S(1)}, u32[]{:S(2)}, u32[]{:S(2)}) collective-permute-start(bf16[32,1024]{1,0:T(8,128)(2,1)S(1)} %get-tuple-element.27), channel_id=1, source_target_pairs={{0,4},{1,5},{2,6},{3,7},{4,0},{5,1},{6,2},{7,3},{8,12},{9,13},{10,... | collective-permute-start | bytes 196616 | tf_op jit(solution)/shard_map/ppermute | solution.py:522
  28.4 6.5 %collective-permute-start.3 = (bf16[32,1024]{1,0:T(8,128)(2,1)S(1)}, bf16[32,1024]{1,0:T(8,128)(2,1)S(1)}, u32[]{:S(2)}, u32[]{:S(2)}) collective-permute-start(bf16[32,1024]{1,0:T(8,128)(2,1)S(1)} %get-tuple-element.27), channel_id=1, source_target_pairs={{0,2},{1,3},{2,4},{3,5},{4,6},{5,7},{6,0},{7,1},{8,10},{9,11},{10,... | collective-permute-start | bytes 196616 | tf_op jit(solution)/shard_map/ppermute | solution.py:522
  35.0 1.4 %collective-permute-start.6 = (f32[32,1024]{1,0:T(8,128)S(1)}, f32[32,1024]{1,0:T(8,128)S(1)}, u32[]{:S(2)}, u32[]{:S(2)}) collective-permute-start(f32[32,1024]{1,0:T(8,128)S(1)} %shard_map.141.one), channel_id=1, source_target_pairs={{0,1},{1,0},{2,3},{3,2},{4,5},{5,4},{6,7},{7,6},{8,9},{9,8},{10,11... | collective-permute-start | bytes 393224 | tf_op jit(solution)/shard_map/ppermute | solution.py:525
  37.2 7.4 %collective-permute-start.9 = (bf16[528,128]{1,0:T(8,128)(2,1)S(1)}, bf16[528,128]{1,0:T(8,128)(2,1)S(1)}, u32[]{:S(2)}, u32[]{:S(2)}) collective-permute-start(bf16[528,128]{1,0:T(8,128)(2,1)S(1)} %get-tuple-element.30.refs_1_), channel_id=1, source_target_pairs={{0,24},{8,16},{16,8},{24,0},{1,25},{9,17},{17,9},{25,1},{2,26},{10... | collective-permute-start | bytes 405512 | tf_op jit(solution)/shard_map/ppermute | solution.py:519
  39.1 7.5 %collective-permute-start.8 = (bf16[528,128]{1,0:T(8,128)(2,1)S(1)}, bf16[528,128]{1,0:T(8,128)(2,1)S(1)}, u32[]{:S(2)}, u32[]{:S(2)}) collective-permute-start(bf16[528,128]{1,0:T(8,128)(2,1)S(1)} %get-tuple-element.30.refs_1_), channel_id=1, source_target_pairs={{0,16},{8,24},{16,0},{24,8},{1,17},{9,25},{17,1},{25,9},{2,18},{10... | collective-permute-start | bytes 405512 | tf_op jit(solution)/shard_map/ppermute | solution.py:519
  40.4 6.3 %collective-permute-start.7 = (bf16[528,128]{1,0:T(8,128)(2,1)S(1)}, bf16[528,128]{1,0:T(8,128)(2,1)S(1)}, u32[]{:S(2)}, u32[]{:S(2)}) collective-permute-start(bf16[528,128]{1,0:T(8,128)(2,1)S(1)} %get-tuple-element.30.refs_1_), channel_id=1, source_target_pairs={{0,8},{8,0},{16,24},{24,16},{1,9},{9,1},{17,25},{25,17},{2,10},{10... | collective-permute-start | bytes 405512 | tf_op jit(solution)/shard_map/ppermute | solution.py:519
  47.5 1.3 %collective-permute-start.10 = (f32[4,32,128]{2,1,0:T(8,128)S(1)}, f32[4,32,128]{2,1,0:T(8,128)S(1)}, u32[]{:S(2)}, u32[]{:S(2)}) collective-permute-start(f32[4,32,128]{2,1,0:T(8,128)S(1)} %get-tuple-element.32), channel_id=1, source_target_pairs={{0,1},{1,0},{2,3},{3,2},{4,5},{5,4},{6,7},{7,6},{8,9},{9,8},{10,11... | collective-permute-start | bytes 196616 | tf_op jit(solution)/shard_map/ppermute | solution.py:525
  48.8 5.5 %collective-permute-start.11 = (bf16[32,128]{1,0:T(8,128)(2,1)S(1)}, bf16[32,128]{1,0:T(8,128)(2,1)S(1)}, u32[]{:S(2)}, u32[]{:S(2)}) collective-permute-start(bf16[32,128]{1,0:T(8,128)(2,1)S(1)} %get-tuple-element.34), channel_id=1, source_target_pairs={{0,2},{1,3},{2,4},{3,5},{4,6},{5,7},{6,0},{7,1},{8,10},{9,11},{10,... | collective-permute-start | bytes 24584 | tf_op jit(solution)/shard_map/ppermute | solution.py:522
  48.8 5.4 %collective-permute-start.12 = (bf16[32,128]{1,0:T(8,128)(2,1)S(1)}, bf16[32,128]{1,0:T(8,128)(2,1)S(1)}, u32[]{:S(2)}, u32[]{:S(2)}) collective-permute-start(bf16[32,128]{1,0:T(8,128)(2,1)S(1)} %get-tuple-element.35), channel_id=1, source_target_pairs={{0,4},{1,5},{2,6},{3,7},{4,0},{5,1},{6,2},{7,3},{8,12},{9,13},{10,... | collective-permute-start | bytes 24584 | tf_op jit(solution)/shard_map/ppermute | solution.py:522
  50.9 4.0 %collective-permute-start.13 = (bf16[32,128]{1,0:T(8,128)(2,1)S(1)}, bf16[32,128]{1,0:T(8,128)(2,1)S(1)}, u32[]{:S(2)}, u32[]{:S(2)}) collective-permute-start(bf16[32,128]{1,0:T(8,128)(2,1)S(1)} %get-tuple-element.36), channel_id=1, source_target_pairs={{0,6},{1,7},{2,0},{3,1},{4,2},{5,3},{6,4},{7,5},{8,14},{9,15},{10,... | collective-permute-start | bytes 24584 | tf_op jit(solution)/shard_map/ppermute | solution.py:522
  (4 other events, 21.5 us)
